TPU v7x, 32 devices: a whole 2x2x4 slice. The times are simulated.
32 devices in a mesh: grp: 2 (over y), fs: 4 (over z), tp: 4 (over x, core).
Axes of the slice: x: 2, y: 2, z: 4, core: 2. Of those that a mesh axis runs over, the one named last changes fastest.
Arguments:
- inputs: bfloat16 [6144, 2048], P(('grp', 'fs'), 'tp'), parts along dimension 0, may hold values from -110 to 110, as said below
- mixer_gain: float32 [2048], replicated, may hold values from 0.1 to 1.9
- query_weight: bfloat16 [2048, 1024], P('fs', 'tp'), may hold values from -0.125 to 0.125
- key_weight: bfloat16 [2048, 1024], P('fs', 'tp'), may hold values from -0.125 to 0.125
- value_weight: bfloat16 [2048, 1024], P('fs', 'tp'), may hold values from -0.125 to 0.125
- gate_weight: bfloat16 [2048, 1024], P('fs', 'tp'), may hold values from -0.125 to 0.125
- head_gain: float32 [1024], P('tp'), may hold values from 0.1 to 1.9
- out_weight: bfloat16 [1024, 2048], P('tp', 'fs'), may hold values from -0.1875 to 0.1875
- channel_gain: float32 [2048], replicated, may hold values from 0.1 to 1.9
- up_weight: bfloat16 [2048, 5632], P('fs', 'tp'), may hold values from -0.125 to 0.125
- switch_weight: bfloat16 [2048, 5632], P('fs', 'tp'), may hold values from -0.125 to 0.125
- filter_up: float32 [3, 5632], P(None, 'tp'), may hold values from -3.5 to 3.5
- filter_switch: float32 [3, 5632], P(None, 'tp'), may hold values from -3.5 to 3.5
- down_weight: bfloat16 [5632, 2048], P('tp', 'fs'), may hold values from -0.078125 to 0.078125
Outputs:
- layer_output: bfloat16 [6144, 2048], P(('grp', 'fs'), 'tp'), parts along dimension 0
There are 2 independent parts, one for each index of `grp`. A program takes and returns all parts, laid end to end along the dimension named above; an argument that names none is the same for every part. Nothing has to cross between parts.
Inputs may be any that keep to these rules, and one draw needn't show every extreme that they name: `inputs`: activations of one part.
All inputs are finite; a program needn't handle non-finite values.
Results may differ from a plain program's by a relative error of at most 0.012.
Values may be sent and summed in bfloat16 or wider, within the bound.
A program may use at most 64 MiB of HBM per device.

v0:
```python
import functools

import jax
import jax.numpy as jnp
from jax import lax
from jax.experimental import pallas as pl
from jax.experimental.pallas import tpu as pltpu
from jax.sharding import PartitionSpec as P

HEAD = 128
EPS = 1e-06
MESH = pl.DeviceIdType.MESH
BF = jnp.bfloat16
F32 = jnp.float32


def chunks_of(rows, most=2):
    while rows % (16 * most):
        most //= 2
    return most


def kernel(cfg, x_hbm, mg, q_hbm, k_hbm, v_hbm, g_hbm, hg, ow_hbm, cg, up_hbm, sw_hbm, fu, fsw, dn_hbm,
           cos_ref, sin_ref, ld_ref, o_ref,
           wq, ob, ub, sb, db, xw, xn, qr, kr, vr, gr, ho, part, ra, st, rb, mw, lift, swit, hid,
           part2, ra2, st2, rb2,
           loc, zs, zr, ys, yr, a1s, a1r, a2s, a2r, b1s, b1r, b2s, b2r, c1s, c1r, c2s, c2r, d1s, d1r, d2s, d2r):
    n_g, n_f, n_t = cfg
    n_x = n_t // 2
    grp, z, t = lax.axis_index("grp"), lax.axis_index("fs"), lax.axis_index("tp")
    x, c = t // 2, t % 2
    partner = x * 2 + (1 - c)
    T, bw = x_hbm.shape
    D = bw * n_t
    RC = 256
    R = T // RC
    width = q_hbm.shape[1]
    heads = width // HEAD
    F = up_hbm.shape[1]
    fr = q_hbm.shape[0]
    slotw = ow_hbm.shape[1]
    per_block = bw // slotw

    def rows_of(r, size=RC):
        return pl.ds(r * size if isinstance(r, int) else pl.multiple_of(r * size, size), size)

    barrier = pltpu.get_barrier_semaphore()
    friends = [(grp, lax.rem(z + 1, n_f), t), (grp, lax.rem(z + n_f - 1, n_f), t), (grp, z, partner)]
    friends += [(lax.rem(grp + d, n_g), z, t) for d in range(1, n_g)]
    friends += [(grp, z, lax.rem(x + d, n_x) * 2 + c) for d in range(1, n_x)]
    for f in friends:
        pl.semaphore_signal(barrier, inc=1, device_id=f, device_id_type=MESH)

    zrow = pl.multiple_of(z * fr, fr)
    local = [pltpu.make_async_copy(x_hbm, xw.at[t], loc.at[0])]
    for i, w in enumerate((q_hbm, k_hbm, v_hbm, g_hbm)):
        local.append(pltpu.make_async_copy(
            w, wq.at[pl.ds(zrow, fr), pl.ds(i * width, width)], loc.at[1 + i]))
    local.append(pltpu.make_async_copy(ow_hbm, ob.at[z], loc.at[5]))
    local.append(pltpu.make_async_copy(up_hbm, ub.at[pl.ds(zrow, fr), :], loc.at[6]))
    local.append(pltpu.make_async_copy(sw_hbm, sb.at[pl.ds(zrow, fr), :], loc.at[7]))
    local.append(pltpu.make_async_copy(dn_hbm, db.at[z], loc.at[8]))
    for cp in local:
        cp.start()

    pending = []

    pieces = []

    def add_pieces(buf, slotted, shard, name):
        half = shard // n_g
        count = 1 if name == "out" else chunks_of(half, 4 if name == "down" else 2)
        size = half // count
        for j in range(count):
            def ref(src, owner, j=j):
                if slotted:
                    lo = owner * half + j * size
                    return buf.at[src, pl.ds(pl.multiple_of(lo, size), size), :]
                lo = src * shard + owner * half + j * size
                return buf.at[pl.ds(pl.multiple_of(lo, size), size), :]
            pieces.append((name, ref))

    add_pieces(wq, False, fr, "qkvg")
    add_pieces(ob, True, ow_hbm.shape[0], "out")
    add_pieces(ub, False, fr, "up")
    add_pieces(sb, False, fr, "switch")
    add_pieces(db, True, dn_hbm.shape[0], "down")
    n_p = len(pieces)

    def z_copy(p, src, step, way):
        ref = pieces[p][1](src, grp)
        return pltpu.make_async_remote_copy(
            src_ref=ref, dst_ref=ref, send_sem=zs.at[p, 2 * step + way], recv_sem=zr.at[p, src],
            device_id=(grp, z + (1 if way == 0 else -1), t), device_id_type=MESH)

    def y_copy(p, src, d):
        ref = pieces[p][1](src, grp)
        return pltpu.make_async_remote_copy(
            src_ref=ref, dst_ref=ref, send_sem=ys.at[p, src * n_g + d], recv_sem=yr.at[p, src * n_g + grp],
            device_id=(lax.rem(grp + d, n_g), z, t), device_id_type=MESH)

    def z_send(p, src, step, way, cond):
        cp = z_copy(p, src, step, way)

        @pl.when(cond)
        def _():
            cp.start()

        pending.append((cond, cp))

    def own(p):
        z_send(p, z, 0, 0, z < n_f - 1)
        z_send(p, z, 0, 1, z > 0)

    def event(p, s):
        for way in (0, 1):
            src = z - s if way == 0 else z + s
            here = (src >= 0) if way == 0 else (src < n_f)
            safe = jnp.clip(src, 0, n_f - 1)

            @pl.when(here)
            def _():
                z_copy(p, safe, s, way).wait_recv()

            onward = jnp.logical_and(here, z < n_f - 1 if way == 0 else z > 0)
            z_send(p, safe, s, way, onward)
            for d in range(1, n_g):
                cp = y_copy(p, safe, d)

                @pl.when(here)
                def _():
                    cp.start()

                pending.append((here, cp))

    def arrive_from(p, src):
        for d in range(1, n_g):
            owner = lax.rem(grp + d, n_g)
            ref = pieces[p][1](src, owner)
            pltpu.make_async_remote_copy(
                src_ref=ref, dst_ref=ref, send_sem=ys.at[p, src * n_g],
                recv_sem=yr.at[p, src * n_g + owner],
                device_id=(owner, z, t), device_id_type=MESH).wait_recv()

    def arrive(p):
        for s in range(1, n_f):
            arrive_from(p, lax.rem(z + s, n_f))

    state = {"own": 0, "ev": 0}
    downs = [i for i, pc in enumerate(pieces) if pc[0] == "down"]
    by_source = per_block == 1
    order = [(p, s) for p in range(n_p) for s in range(1, n_f) if not (by_source and p in downs)]
    if by_source:
        order += [(p, s) for s in range(1, n_f) for p in downs]

    def send_own(upto):
        while state["own"] < min(upto, n_p):
            own(state["own"])
            state["own"] += 1

    def pump(count=1):
        for _ in range(count):
            if state["ev"] < len(order):
                p, s = order[state["ev"]]
                send_own(p + 3)
                event(p, s)
                state["ev"] += 1

    def pump_through(name):
        last = max(i for i, pc in enumerate(pieces) if pc[0] == name)
        while state["ev"] < len(order) and order[state["ev"]][0] <= last:
            pump()

    def arrive_all(name):
        pump_through(name)
        for i, pc in enumerate(pieces):
            if pc[0] == name:
                arrive(i)

    def ag_copy(buf, src_x, r, dest, ssem, rsem):
        ref = buf.at[src_x * 2 + c, rows_of(r), :]
        return pltpu.make_async_remote_copy(
            src_ref=ref, dst_ref=ref, send_sem=ssem, recv_sem=rsem,
            device_id=(grp, z, dest), device_id_type=MESH)

    def go(cp):
        cp.start()
        pending.append((None, cp))

    def ag_start(buf, r, sems):
        s1, r1, s2, r2 = sems
        for d in range(1, n_x):
            go(ag_copy(buf, x, r, lax.rem(x + d, n_x) * 2 + c, s1.at[d, r], r1.at[x, r]))
        go(ag_copy(buf, x, r, partner, s2.at[x, r], r2.at[x, r]))

    def ag_forward(buf, r, sems):
        s1, r1, s2, r2 = sems
        for d in range(1, n_x):
            sx = lax.rem(x + d, n_x)
            ag_copy(buf, sx, r, partner, s1.at[d, r], r1.at[sx, r]).wait_recv()
            go(ag_copy(buf, sx, r, partner, s2.at[sx, r], r2.at[sx, r]))

    def ag_finish(buf, r, sems):
        s1, r1, s2, r2 = sems
        for sx in range(n_x):
            ref = buf.at[sx * 2 + (1 - c), rows_of(r), :]
            pltpu.make_async_remote_copy(
                src_ref=ref, dst_ref=ref, send_sem=s2.at[sx, r], recv_sem=r2.at[sx, r],
                device_id=(grp, z, partner), device_id_type=MESH).wait_recv()

    def norm_rows(src, gain, r):
        def body(i, _):
            rows = rows_of(r * (RC // 64) + i, 64)
            total = jnp.zeros((64, 1), F32)
            for b in range(n_t):
                val = src[b, rows, :].astype(F32)
                total = total + jnp.sum(val * val, axis=-1, keepdims=True)
            inv = lax.rsqrt(total / D + EPS)
            for b in range(n_t):
                val = src[b, rows, :].astype(F32)
                xn[rows, b * bw:(b + 1) * bw] = (val * inv * gain[:, b * bw:(b + 1) * bw]).astype(BF)
            return 0
        lax.fori_loop(0, RC // 64, body, 0)

    def product(lhs, rhs, dst, block, r):
        for j in range(per_block):
            dst[block, rows_of(r), j * slotw:(j + 1) * slotw] = jnp.dot(
                lhs[rows_of(r), :], rhs[block * per_block + j], preferred_element_type=F32).astype(BF)

    def rs_copy(src_ref, dst_ref, dest, ssem, rsem):
        return pltpu.make_async_remote_copy(
            src_ref=src_ref, dst_ref=dst_ref, send_sem=ssem, recv_sem=rsem,
            device_id=(grp, z, dest), device_id_type=MESH)

    def reduce(lhs, rhs, prt, r_a, stage, r_b, sems, base, emit):
        s1, r1, s2, r2 = sems

        def to_partner(d, r):
            bx = lax.rem(x + d, n_x)
            return rs_copy(prt.at[bx * 2 + 1 - c, rows_of(r), :], r_a.at[d, rows_of(r), :],
                           partner, s1.at[d, r], r1.at[d, r])

        def across(d, r):
            return rs_copy(stage.at[d, rows_of(r), :], r_b.at[d, rows_of(r), :],
                           lax.rem(x + d, n_x) * 2 + c, s2.at[d, r], r2.at[d, r])

        def combine(d, r):
            bx = lax.rem(x + d, n_x)
            to_partner(d, r).wait_recv()
            stage[d, rows_of(r), :] = (prt[bx * 2 + c, rows_of(r), :].astype(F32)
                                       + r_a[d, rows_of(r), :].astype(F32)).astype(BF)
            go(across(d, r))

        work = [(d, r) for d in range(1, n_x) for r in range(R)]
        prev = None
        for d, r in work + [(0, r) for r in range(R)]:
            bx = lax.rem(x + d, n_x)
            product(lhs, rhs, prt, bx * 2 + 1 - c, r)
            go(to_partner(d, r))
            product(lhs, rhs, prt, bx * 2 + c, r)
            if prev is not None and prev[0] > 0:
                combine(*prev)
            prev = (d, r)
            if r % 2 == 1:
                pump(1)
        for r in range(R):
            pump(1)
            to_partner(0, r).wait_recv()
            total = prt[t, rows_of(r), :].astype(F32) + r_a[0, rows_of(r), :].astype(F32)
            for d in range(1, n_x):
                across(d, r).wait_recv()
                total = total + r_b[d, rows_of(r), :].astype(F32)
            emit(r, (base[t, rows_of(r), :].astype(F32) + total).astype(BF))

    pl.semaphore_wait(barrier, len(friends))
    local[0].wait()
    agx = (a1s, a1r, a2s, a2r)
    for r in range(R):
        ag_start(xw, r, agx)
    for cp in local[1:]:
        cp.wait()
    send_own(2)
    pump(1)
    for r in range(R):
        ag_forward(xw, r, agx)
    pump(1)
    for r in range(R):
        ag_finish(xw, r, agx)
        norm_rows(xw, mg, r)
        pump(1)
    arrive_all("qkvg")
    send_own(5)

    def project(r, _):
        rows = rows_of(r)
        lhs = xn[rows, :]
        for i, dst in enumerate((qr, kr, vr, gr)):
            val = jnp.dot(lhs, wq[:, i * width:(i + 1) * width], preferred_element_type=F32).astype(BF)
            if i >= 2:
                dst[rows, :] = val
                continue
            for h in range(heads):
                part_h = val[:, h * HEAD:(h + 1) * HEAD].astype(F32)
                dst[rows, h * HEAD:(h + 1) * HEAD] = (
                    part_h * cos_ref[rows, :] + pltpu.roll(part_h, HEAD // 2, 1) * sin_ref[rows, :]).astype(BF)
        return 0

    for r in range(R):
        project(r, 0)
        pump(1)
    for h in range(heads):
        cols = slice(h * HEAD, (h + 1) * HEAD)
        for r in range(R):
            span = (r + 1) * RC
            qh = qr[r * RC:(r + 1) * RC, cols]
            scores = lax.dot_general(qh, kr[0:span, cols], (((1,), (1,)), ((), ())),
                                     preferred_element_type=F32)
            gap = (r * RC + lax.broadcasted_iota(jnp.int32, (RC, span), 0)
                   - lax.broadcasted_iota(jnp.int32, (RC, span), 1))
            causal = gap >= 0
            rate = ld_ref[h:h + 1, 0:1]
            fade = jnp.where(causal, jnp.exp(rate * jnp.where(causal, gap, 0).astype(F32)), 0.0)
            weights = (scores * HEAD ** (-0.5) * fade).astype(BF)
            kept = jnp.dot(weights, vr[0:span, cols], preferred_element_type=F32)
            kept = kept * lax.rsqrt(jnp.mean(kept * kept, axis=-1, keepdims=True) + EPS)
            gate = gr[r * RC:(r + 1) * RC, cols].astype(F32)
            ho[r * RC:(r + 1) * RC, cols] = (kept * hg[:, cols] * (gate / (1.0 + jnp.exp(-gate)))).astype(BF)
            if r != 1:
                pump(1)
    arrive_all("out")
    agm = (c1s, c1r, c2s, c2r)

    def emit_mixed(r, val):
        mw[t, rows_of(r), :] = val
        ag_start(mw, r, agm)

    reduce(ho, ob, part, ra, st, rb, (b1s, b1r, b2s, b2r), xw, emit_mixed)
    for r in range(R):
        ag_forward(mw, r, agm)
        if r % 2 == 0:
            pump(1)
    for r in range(R):
        ag_finish(mw, r, agm)
        norm_rows(mw, cg, r)
        pump(1)
    arrive_all("up")

    lift[0:16, :] = jnp.zeros((16, F), BF)
    swit[0:16, :] = jnp.zeros((16, F), BF)

    def widen(weights, dst, r):
        dst[pl.ds(16 + r * RC, RC), :] = jnp.dot(
            xn[rows_of(r), :], weights[...], preferred_element_type=F32).astype(BF)

    for r in range(R):
        widen(ub, lift, r)
        pump(1)
    arrive_all("switch")
    edges = list(range(0, F, 256)) + [F]

    def conv_rows(i, _):
        for lo, hi in zip(edges[:-1], edges[1:]):
            mixed = []
            for src, taps in ((lift, fu), (swit, fsw)):
                val = src[pl.ds(pl.multiple_of(i * 64, 64), 80), lo:hi].astype(F32)
                acc = pltpu.roll(val, 2, 0)[16:] * taps[0:1, lo:hi]
                acc = acc + pltpu.roll(val, 1, 0)[16:] * taps[1:2, lo:hi]
                mixed.append(acc + val[16:] * taps[2:3, lo:hi])
            a, b = mixed
            hid[rows_of(i, 64), lo:hi] = (a * (b / (1.0 + jnp.exp(-b)))).astype(BF)
        return 0

    for r in range(R):
        widen(sb, swit, r)
        pump(1)
        for part_r in range(2):
            first = r * (RC // 64) + part_r * (RC // 128)
            lax.fori_loop(first, first + RC // 128, conv_rows, 0)
            pump(1)

    def emit_out(r, val):
        o_ref[rows_of(r), :] = val

    def slot_reduce(s, way):
        slot = z - s if way == 0 else z + s
        here = (slot >= 0) if way == 0 else (slot < n_f)
        b = jnp.clip(slot, 0, n_f - 1)
        bx, bc = b // 2, b % 2
        d = lax.rem(bx - x + n_x, n_x)
        to_other = jnp.logical_and(here, bc != c)
        relay = jnp.logical_and(jnp.logical_and(here, bc == c), bx != x)
        if s > 0:
            @pl.when(here)
            def _():
                for p in downs:
                    arrive_from(p, b)
        ups, outs = [], []
        for r in range(R):
            up = rs2(part2.at[b, rows_of(r), :], ra2.at[d, rows_of(r), :], partner, d1s.at[d, r], d1r.at[d, r])
            out = rs2(st2.at[d, rows_of(r), :], rb2.at[d, rows_of(r), :], bx * 2 + c, d2s.at[d, r], d2r.at[d, r])
            pending.append((to_other, up))
            pending.append((relay, out))
            ups.append(up)
            outs.append(out)

        for r in range(R):
            @pl.when(here)
            def _(r=r):
                product(hid, db, part2, b, r)

            @pl.when(to_other)
            def _(r=r):
                ups[r].start()

        def second():
            for r in range(R):
                @pl.when(relay)
                def _(r=r):
                    ups[r].wait_recv()
                    st2[d, rows_of(r), :] = (part2[b, rows_of(r), :].astype(F32)
                                             + ra2[d, rows_of(r), :].astype(F32)).astype(BF)
                    outs[r].start()
        return second

    rs2 = rs_copy
    if by_source:
        slot_reduce(0, 0)()
        for s in range(1, n_f):
            while state["ev"] < len(order) and order[state["ev"]][1] <= s:
                pump()
            later = [slot_reduce(s, way) for way in (0, 1)]
            for act in later:
                act()
        for r in range(R):
            rs2(part2.at[t, rows_of(r), :], ra2.at[0, rows_of(r), :], partner, d1s.at[0, r], d1r.at[0, r]).wait_recv()
            total = part2[t, rows_of(r), :].astype(F32) + ra2[0, rows_of(r), :].astype(F32)
            for d in range(1, n_x):
                rs2(st2.at[d, rows_of(r), :], rb2.at[d, rows_of(r), :], lax.rem(x + d, n_x) * 2 + c,
                    d2s.at[d, r], d2r.at[d, r]).wait_recv()
                total = total + rb2[d, rows_of(r), :].astype(F32)
            emit_out(r, (mw[t, rows_of(r), :].astype(F32) + total).astype(BF))
    else:
        arrive_all("down")
        reduce(hid, db, part2, ra2, st2, rb2, (d1s, d1r, d2s, d2r), mw, emit_out)

    for cond, cp in pending:
        if cond is None:
            cp.wait_send()
        else:
            @pl.when(cond)
            def _(cp=cp):
                cp.wait_send()


def on_device(cfg, inputs, mixer_gain, query_weight, key_weight, value_weight, gate_weight, head_gain,
              out_weight, channel_gain, up_weight, switch_weight, filter_up, filter_switch, down_weight):
    n_g, n_f, n_t = cfg
    n_x = n_t // 2
    T, bw = inputs.shape
    D = bw * n_t
    fr, width = query_weight.shape
    heads = width // HEAD
    F = up_weight.shape[1]
    slotw = out_weight.shape[1]
    half = HEAD // 2
    frequency = 10000.0 ** (-jnp.arange(half, dtype=F32) * 2.0 / HEAD)
    angles = jnp.arange(T, dtype=jnp.int32).astype(F32)[:, None] * frequency[None, :]
    cosine, sine = jnp.cos(angles), jnp.sin(angles)
    cos2 = jnp.concatenate([cosine, cosine], axis=1)
    sin2 = jnp.concatenate([-sine, sine], axis=1)
    ids = (lax.axis_index("tp") * heads + jnp.arange(heads, dtype=jnp.int32)).astype(F32)
    rate = jnp.broadcast_to(jnp.log1p(-jnp.exp2(-5.0 - ids))[:, None], (heads, 128))

    n_p = (chunks_of(fr // n_g) * 3 + 1 + chunks_of(down_weight.shape[0] // n_g, 4))
    R = T // 256
    dma = pltpu.SemaphoreType.DMA
    anyspec = pl.BlockSpec(memory_space=pl.ANY)
    vspec = pl.BlockSpec(memory_space=pltpu.VMEM)
    tp_sems = [dma((n_x, R))] * 16
    act = pltpu.VMEM((n_t, T, bw), BF)
    xblk = pltpu.VMEM((n_x, T, bw), BF)
    scratch = [
        pltpu.VMEM((D, 4 * width), BF),
        pltpu.VMEM((n_f,) + out_weight.shape, BF),
        pltpu.VMEM((D, F), BF),
        pltpu.VMEM((D, F), BF),
        pltpu.VMEM((n_f,) + down_weight.shape, BF),
        act,
        pltpu.VMEM((T, D), BF),
        pltpu.VMEM((T, width), BF), pltpu.VMEM((T, width), BF),
        pltpu.VMEM((T, width), BF), pltpu.VMEM((T, width), BF),
        pltpu.VMEM((T, width), BF),
        act, xblk, xblk, xblk,
        act,
        pltpu.VMEM((T + 16, F), BF), pltpu.VMEM((T + 16, F), BF), pltpu.VMEM((T, F), BF),
        act, xblk, xblk, xblk,
        dma((9,)),
        dma((n_p, 2 * n_f)), dma((n_p, n_f)), dma((n_p, n_f * n_g)), dma((n_p, n_f * n_g)),
    ] + tp_sems
    flops = 2 * T * (D * 4 * width + width * D + 3 * D * F)
    call = pl.pallas_call(
        functools.partial(kernel, cfg),
        out_shape=jax.ShapeDtypeStruct((T, bw), BF),
        in_specs=[anyspec, vspec, anyspec, anyspec, anyspec, anyspec, vspec, anyspec, vspec, anyspec, anyspec,
                  vspec, vspec, anyspec, vspec, vspec, vspec],
        out_specs=vspec,
        scratch_shapes=scratch,
        compiler_params=pltpu.CompilerParams(
            collective_id=0, has_side_effects=True, vmem_limit_bytes=67043328),
        cost_estimate=pl.CostEstimate(flops=flops, bytes_accessed=2 * (D * F * 3), transcendentals=0),
    )
    return call(inputs, mixer_gain[None, :], query_weight, key_weight, value_weight, gate_weight,
                head_gain[None, :], out_weight, channel_gain[None, :], up_weight, switch_weight,
                filter_up, filter_switch, down_weight, cos2, sin2, rate)


def solution(mesh):
    cfg = (mesh.shape["grp"], mesh.shape["fs"], mesh.shape["tp"])
    return jax.shard_map(
        functools.partial(on_device, cfg),
        mesh=mesh,
        in_specs=(
            P(("grp", "fs"), "tp"),
            P(),
            P("fs", "tp"),
            P("fs", "tp"),
            P("fs", "tp"),
            P("fs", "tp"),
            P("tp"),
            P("tp", "fs"),
            P(),
            P("fs", "tp"),
            P("fs", "tp"),
            P(None, "tp"),
            P(None, "tp"),
            P("tp", "fs"),
        ),
        out_specs=P(("grp", "fs"), "tp"),
        check_vma=False,
    )
```

profile of v0, /device:TPU:3, one launch (start us, length us, event | category | flops | bytes accessed | tf_op | source)
XLA Modules:
  0.0 235.7 jit_solution(2523855198774405907)
XLA Ops:
  0.0 1.5 fusion
  1.5 1.1 pad_maximum_fusion
  2.6 0.6 broadcast_in_dim.20.ld_ref
  3.2 230.4 %shard_map.136 = bf16[768,512]{1,0:T(8,128)(2,1)} custom-call(bf16[768,512]{1,0:T(8,128)(2,1)} %x_hbm.1, f32[1,2048]{1,0:T(1,128)} %bitcast.3, bf16[512,256]{1,0:T(8,128)(2,1)} %q_hbm.1, bf16[512,256]{1,0:T(8,128)(2,1)} %k_hbm.1, bf16[512,256]{1,0:T(8,128)(2,1)} %v_hbm.1, bf16[512,256]{1,0:T(8,128)(2,1)} %g_hbm.1, f32[1,256]{1,0:T(1,128)} %bitcast.5, ...), custom_call_target="tpu_custom_call" | custom-call | flops 17314086912 | bytes 17301504 | tf_op jit(solution)/shard_map/pallas_call | solution.py:512
  233.6 2.1 copy.16
  (3 shorter events, 0.0 us)
where the time goes:
time: 236 us
  Pallas kernels  230 us (97%)
  local copies, waits for them, and re-layouts  2.68 us (1%)
  other arithmetic  2.62 us (1%)
    pallas_call x1, Pallas kernels, on_device(): call(inputs, mixer_gain[None, :], query_weight, key_weight, value_weight,...  230 us

commit v1 on v0

v1 whole, which is shorter than its diff:
```python
import functools

import jax
import jax.numpy as jnp
from jax import lax
from jax.experimental import pallas as pl
from jax.experimental.pallas import tpu as pltpu
from jax.sharding import PartitionSpec as P

HEAD = 128
EPS = 1e-06
MESH = pl.DeviceIdType.MESH
BF = jnp.bfloat16
F32 = jnp.float32
LEAD = 3


def hidden_chunks(hidden):
    if hidden % 128:
        return [(0, hidden)]
    edges = list(range(0, hidden, 512)) + [hidden]
    return list(zip(edges[:-1], edges[1:]))


def kernel(cfg, x_hbm, mg, q_hbm, k_hbm, v_hbm, g_hbm, hg, ow_hbm, cg, up_hbm, sw_hbm, fu, fsw, dn_hbm,
           cos_ref, sin_ref, ld_ref, o_ref, *scratch):
    (wq, ob, ub, sb, db, xw, xn, xn1, qr, kr, vr, gr, ho, part, ra, st, rb, mw, mw1, lift, swit, hid,
     part1, ra1, st1, rb1, fin, loc, zs, zr, ys, yr, tks, tkr, fns, fnr) = scratch[:36]
    agx, agm, agn, rsm, rs0, rs1 = [scratch[36 + 4 * i:40 + 4 * i] for i in range(6)]
    n_g, n_f, n_t = cfg
    n_x = n_t // 2
    grp, z, t = lax.axis_index("grp"), lax.axis_index("fs"), lax.axis_index("tp")
    x, c = t // 2, t % 2
    partner = x * 2 + (1 - c)
    T, bw = x_hbm.shape
    D = bw * n_t
    RC = 256
    R = T // RC
    width = q_hbm.shape[1]
    heads = width // HEAD
    F = up_hbm.shape[1]
    fr = q_hbm.shape[0]
    slotw = ow_hbm.shape[1]
    per_block = bw // slotw
    n_j = slotw // 128
    w_j = per_block * 128
    chunks = hidden_chunks(F)

    is_end = jnp.logical_or(z == 0, z == n_f - 1)
    inner = jnp.logical_not(is_end)
    host = jnp.where(z == 0, 1, n_f - 2)
    guest = jnp.where(z == 1, 0, n_f - 1)
    second = None if n_f == 4 else jnp.logical_or(z == 1, z == n_f - 2)

    def when(cond):
        if cond is None:
            return lambda f: f()
        return pl.when(cond)

    def rows_of(r, size=RC):
        return pl.ds(r * size if isinstance(r, int) else pl.multiple_of(r * size, size), size)

    barrier = pltpu.get_barrier_semaphore()
    friends = [(grp, lax.rem(z + 1, n_f), t), (grp, lax.rem(z + n_f - 1, n_f), t), (grp, z, partner)]
    friends += [(lax.rem(grp + d, n_g), z, t) for d in range(1, n_g)]
    friends += [(grp, z, lax.rem(x + d, n_x) * 2 + c) for d in range(1, n_x)]
    for f in friends:
        pl.semaphore_signal(barrier, inc=1, device_id=f, device_id_type=MESH)

    zrow = pl.multiple_of(z * fr, fr)
    zcol = pl.multiple_of(z * 128, 128)
    local = [pltpu.make_async_copy(x_hbm, xw.at[t], loc.at[0])]
    for i, w in enumerate((q_hbm, k_hbm, v_hbm, g_hbm)):
        local.append(pltpu.make_async_copy(
            w, wq.at[pl.ds(zrow, fr), pl.ds(i * width, width)], loc.at[1 + i]))
    local.append(pltpu.make_async_copy(ow_hbm, ob.at[z], loc.at[5]))
    local.append(pltpu.make_async_copy(up_hbm, ub.at[pl.ds(zrow, fr), :], loc.at[6]))
    local.append(pltpu.make_async_copy(sw_hbm, sb.at[pl.ds(zrow, fr), :], loc.at[7]))
    for j in range(n_j):
        local.append(pltpu.make_async_copy(
            dn_hbm.at[:, pl.ds(j * 128, 128)], db.at[j, :, pl.ds(zcol, 128)], loc.at[8 + j]))
    for cp in local:
        cp.start()

    open_copies = [[]]

    def go(cp, cond=None):
        when(cond)(cp.start)
        open_copies[-1].append((cond, cp))

    def recv(cp, cond=None):
        when(cond)(cp.wait_recv)

    def drain():
        for cond, cp in open_copies[-1]:
            when(cond)(cp.wait_send)
        open_copies[-1].clear()

    pieces = []

    def add_rows(name, buf, slotted, shard, cols=None):
        half = shard // n_g
        count = 2 if name == "qkvg" and half % 32 == 0 else 1
        size = half // count
        for j in range(count):
            def ref(src, owner, j=j):
                if slotted:
                    return buf.at[src, pl.ds(pl.multiple_of(owner * half + j * size, size), size), :]
                rows = pl.ds(pl.multiple_of(src * shard + owner * half + j * size, size), size)
                return buf.at[rows, :] if cols is None else buf.at[rows, pl.ds(cols[0], cols[1] - cols[0])]
            pieces.append((name, ref))

    add_rows("qkvg", wq, False, fr)
    add_rows("out", ob, True, ow_hbm.shape[0])
    for k, cols in enumerate(chunks):
        for buf in (ub, sb):
            add_rows("ff%d" % k, buf, False, fr, cols if len(chunks) > 1 else None)
    for j in range(n_j):
        def down_ref(src, owner, j=j):
            half = F // n_g
            return db.at[j, pl.ds(pl.multiple_of(owner * half, half), half),
                         pl.ds(pl.multiple_of(src * 128, 128), 128)]
        pieces.append(("down%d" % j, down_ref))
    n_p = len(pieces)
    first_ff = min(i for i, pc in enumerate(pieces) if pc[0] == "ff0")

    def z_copy(p, src, step, way):
        ref = pieces[p][1](src, grp)
        return pltpu.make_async_remote_copy(
            src_ref=ref, dst_ref=ref, send_sem=zs.at[p, 2 * step + way], recv_sem=zr.at[p, src],
            device_id=(grp, z + (1 if way == 0 else -1), t), device_id_type=MESH)

    def y_copy(p, src, d):
        ref = pieces[p][1](src, grp)
        return pltpu.make_async_remote_copy(
            src_ref=ref, dst_ref=ref, send_sem=ys.at[p, src * n_g + d], recv_sem=yr.at[p, src * n_g + grp],
            device_id=(lax.rem(grp + d, n_g), z, t), device_id_type=MESH)

    def other_half(p, d):
        owner = lax.rem(grp + d, n_g)
        ref = pieces[p][1](z, owner)
        return pltpu.make_async_remote_copy(
            src_ref=ref, dst_ref=ref, send_sem=ys.at[p, z * n_g + d], recv_sem=yr.at[p, z * n_g + owner],
            device_id=(grp, host, t), device_id_type=MESH)

    def onward(p, way):
        edge = 1 if p >= first_ff else 0
        return z < n_f - 1 - edge if way == 0 else z > edge

    def own(p):
        for way in (0, 1):
            go(z_copy(p, z, 0, way), onward(p, way))
        if p >= first_ff:
            for d in range(1, n_g):
                go(other_half(p, d), is_end)

    def event(p, s):
        feed = p >= first_ff
        for way in (0, 1):
            src = z - s if way == 0 else z + s
            here = (src >= 0) if way == 0 else (src < n_f)
            if feed:
                here = jnp.logical_and(here, inner)
            safe = jnp.clip(src, 0, n_f - 1)
            recv(z_copy(p, safe, s, way), here)
            go(z_copy(p, safe, s, way), jnp.logical_and(here, onward(p, way)))
            share = here
            if feed and s == 1:
                share = jnp.logical_and(here, z != (1 if way == 0 else n_f - 2))
            for d in range(1, n_g):
                go(y_copy(p, safe, d), share)

    def arrive(p):
        for s in range(1, n_f):
            src = lax.rem(z + s, n_f)
            for d in range(1, n_g):
                owner = lax.rem(grp + d, n_g)
                ref = pieces[p][1](src, owner)
                pltpu.make_async_remote_copy(
                    src_ref=ref, dst_ref=ref, send_sem=ys.at[p, src * n_g],
                    recv_sem=yr.at[p, src * n_g + owner],
                    device_id=(owner, z, t), device_id_type=MESH).wait_recv()

    state = {"own": 0, "ev": 0}
    order = [(p, s) for p in range(n_p) for s in range(1, n_f - 1 if p >= first_ff else n_f)]

    def send_own(upto):
        while state["own"] < min(upto, n_p):
            own(state["own"])
            state["own"] += 1

    def pump(count=1):
        for _ in range(count):
            if state["ev"] < len(order):
                p, s = order[state["ev"]]
                send_own(p + LEAD)
                event(p, s)
                state["ev"] += 1

    def arrive_all(name):
        last = max(i for i, pc in enumerate(pieces) if pc[0] == name)
        while state["ev"] < len(order) and order[state["ev"]][0] <= last:
            pump()
        for i, pc in enumerate(pieces):
            if pc[0] == name:
                arrive(i)

    def ag_copy(buf, src_x, r, dest, ssem, rsem):
        ref = buf.at[src_x * 2 + c, rows_of(r), :]
        return pltpu.make_async_remote_copy(
            src_ref=ref, dst_ref=ref, send_sem=ssem, recv_sem=rsem,
            device_id=(grp, z, dest), device_id_type=MESH)

    def ag_start(buf, r, sems, cond=None):
        s1, r1, s2, r2 = sems
        for d in range(1, n_x):
            go(ag_copy(buf, x, r, lax.rem(x + d, n_x) * 2 + c, s1.at[d, r], r1.at[x, r]), cond)
        go(ag_copy(buf, x, r, partner, s2.at[x, r], r2.at[x, r]), cond)

    def ag_forward(buf, r, sems, cond=None):
        s1, r1, s2, r2 = sems
        for d in range(1, n_x):
            sx = lax.rem(x + d, n_x)
            recv(ag_copy(buf, sx, r, partner, s1.at[d, r], r1.at[sx, r]), cond)
            go(ag_copy(buf, sx, r, partner, s2.at[sx, r], r2.at[sx, r]), cond)

    def ag_finish(buf, r, sems, cond=None):
        s1, r1, s2, r2 = sems
        for sx in range(n_x):
            ref = buf.at[sx * 2 + (1 - c), rows_of(r), :]
            recv(pltpu.make_async_remote_copy(
                src_ref=ref, dst_ref=ref, send_sem=s2.at[sx, r], recv_sem=r2.at[sx, r],
                device_id=(grp, z, partner), device_id_type=MESH), cond)

    def norm_rows(src, gain, r, dst):
        def body(i, _):
            rows = rows_of(r * (RC // 64) + i, 64)
            total = jnp.zeros((64, 1), F32)
            for b in range(n_t):
                val = src[b, rows, :].astype(F32)
                total = total + jnp.sum(val * val, axis=-1, keepdims=True)
            inv = lax.rsqrt(total / D + EPS)
            for b in range(n_t):
                val = src[b, rows, :].astype(F32)
                dst[rows, b * bw:(b + 1) * bw] = (val * inv * gain[:, b * bw:(b + 1) * bw]).astype(BF)
            return 0
        lax.fori_loop(0, RC // 64, body, 0)

    def product(lhs, rhs, dst, block, r):
        for j in range(per_block):
            dst[block, rows_of(r), j * slotw:(j + 1) * slotw] = jnp.dot(
                lhs[rows_of(r), :], rhs[block * per_block + j], preferred_element_type=F32).astype(BF)

    def rs_copy(src_ref, dst_ref, dest, ssem, rsem):
        return pltpu.make_async_remote_copy(
            src_ref=src_ref, dst_ref=dst_ref, send_sem=ssem, recv_sem=rsem,
            device_id=(grp, z, dest), device_id_type=MESH)

    def mixer_reduce(emit):
        s1, r1, s2, r2 = rsm

        def to_partner(d, r):
            bx = lax.rem(x + d, n_x)
            return rs_copy(part.at[bx * 2 + 1 - c, rows_of(r), :], ra.at[d, rows_of(r), :],
                           partner, s1.at[d, r], r1.at[d, r])

        def across(d, r):
            return rs_copy(st.at[d - 1, rows_of(r), :], rb.at[d - 1, rows_of(r), :],
                           lax.rem(x + d, n_x) * 2 + c, s2.at[d, r], r2.at[d, r])

        sends = []

        def begin(cp):
            cp.start()
            sends.append(cp)

        def combine(d, r):
            bx = lax.rem(x + d, n_x)
            to_partner(d, r).wait_recv()
            st[d - 1, rows_of(r), :] = (part[bx * 2 + c, rows_of(r), :].astype(F32)
                                        + ra[d, rows_of(r), :].astype(F32)).astype(BF)
            begin(across(d, r))

        work = [(d, r) for d in range(1, n_x) for r in range(R)]
        prev = None
        for d, r in work + [(0, r) for r in range(R)]:
            bx = lax.rem(x + d, n_x)
            product(ho, ob, part, bx * 2 + 1 - c, r)
            begin(to_partner(d, r))
            product(ho, ob, part, bx * 2 + c, r)
            if prev is not None and prev[0] > 0:
                combine(*prev)
            prev = (d, r)
            if r % 2 == 1:
                pump(1)
        for r in range(R):
            pump(1)
            to_partner(0, r).wait_recv()
            total = part[t, rows_of(r), :].astype(F32) + ra[0, rows_of(r), :].astype(F32)
            for d in range(1, n_x):
                across(d, r).wait_recv()
                total = total + rb[d - 1, rows_of(r), :].astype(F32)
            emit(r, (xw[t, rows_of(r), :].astype(F32) + total).astype(BF))
        for cp in sends:
            cp.wait_send()

    pl.semaphore_wait(barrier, len(friends))
    local[0].wait()
    for r in range(R):
        ag_start(xw, r, agx)
    for cp in local[1:]:
        cp.wait()
    send_own(2)
    pump(1)
    for r in range(R):
        ag_forward(xw, r, agx)
    pump(1)
    for r in range(R):
        ag_finish(xw, r, agx)
        norm_rows(xw, mg, r, xn)
        pump(1)
    arrive_all("qkvg")
    send_own(5)

    def project(r):
        rows = rows_of(r)
        lhs = xn[rows, :]
        for i, dst in enumerate((qr, kr, vr, gr)):
            val = jnp.dot(lhs, wq[:, i * width:(i + 1) * width], preferred_element_type=F32).astype(BF)
            if i >= 2:
                dst[rows, :] = val
                continue
            for h in range(heads):
                part_h = val[:, h * HEAD:(h + 1) * HEAD].astype(F32)
                dst[rows, h * HEAD:(h + 1) * HEAD] = (
                    part_h * cos_ref[rows, :] + pltpu.roll(part_h, HEAD // 2, 1) * sin_ref[rows, :]).astype(BF)

    for r in range(R):
        project(r)
        pump(1)
    for h in range(heads):
        cols = slice(h * HEAD, (h + 1) * HEAD)
        for r in range(R):
            span = (r + 1) * RC
            qh = qr[r * RC:(r + 1) * RC, cols]
            scores = lax.dot_general(qh, kr[0:span, cols], (((1,), (1,)), ((), ())),
                                     preferred_element_type=F32)
            gap = (r * RC + lax.broadcasted_iota(jnp.int32, (RC, span), 0)
                   - lax.broadcasted_iota(jnp.int32, (RC, span), 1))
            causal = gap >= 0
            rate = ld_ref[h:h + 1, 0:1]
            fade = jnp.where(causal, jnp.exp(rate * jnp.where(causal, gap, 0).astype(F32)), 0.0)
            weights = (scores * HEAD ** (-0.5) * fade).astype(BF)
            kept = jnp.dot(weights, vr[0:span, cols], preferred_element_type=F32)
            kept = kept * lax.rsqrt(jnp.mean(kept * kept, axis=-1, keepdims=True) + EPS)
            gate = gr[r * RC:(r + 1) * RC, cols].astype(F32)
            ho[r * RC:(r + 1) * RC, cols] = (kept * hg[:, cols] * (gate / (1.0 + jnp.exp(-gate)))).astype(BF)
            if r != 1:
                pump(1)
    arrive_all("out")

    def token_copy(r, dest):
        return pltpu.make_async_remote_copy(
            src_ref=mw.at[t, rows_of(r), :], dst_ref=mw1.at[t, rows_of(r), :],
            send_sem=tks.at[r], recv_sem=tkr.at[r], device_id=(grp, dest, t), device_id_type=MESH)

    def emit_mixed(r, val):
        mw[t, rows_of(r), :] = val
        go(token_copy(r, host), is_end)
        ag_start(mw, r, agm, inner)

    mixer_reduce(emit_mixed)

    def fin_copy(j, dest):
        return pltpu.make_async_remote_copy(
            src_ref=fin.at[j], dst_ref=fin.at[j], send_sem=fns.at[j], recv_sem=fnr.at[j],
            device_id=(grp, dest, t), device_id_type=MESH)

    def cols_of(j):
        return slice(j * w_j, (j + 1) * w_j)

    def end_part():
        open_copies.append([])
        send_own(n_p)
        for j in range(n_j):
            fin_copy(j, host).wait_recv()
            o_ref[:, cols_of(j)] = fin[j]
        drain()
        open_copies.pop()

    def widen(weights, lhs, dst, k):
        lo, hi = chunks[k]

        def body(r, _):
            dst[pl.ds(pl.multiple_of(16 + r * RC, 16), RC), 0:hi - lo] = jnp.dot(
                lhs[rows_of(r), :], weights[:, lo:hi], preferred_element_type=F32).astype(BF)
            return 0
        lax.fori_loop(0, R, body, 0)

    def conv(q, k):
        first, last = chunks[k]
        edges = list(range(0, last - first, 256)) + [last - first]

        def body(i, _):
            for lo, hi in zip(edges[:-1], edges[1:]):
                mixed = []
                for src, taps in ((lift, fu), (swit, fsw)):
                    val = src[pl.ds(pl.multiple_of(i * 64, 64), 80), lo:hi].astype(F32)
                    acc = pltpu.roll(val, 2, 0)[16:] * taps[0:1, first + lo:first + hi]
                    acc = acc + pltpu.roll(val, 1, 0)[16:] * taps[1:2, first + lo:first + hi]
                    mixed.append(acc + val[16:] * taps[2:3, first + lo:first + hi])
                a, b = mixed
                hid[q, rows_of(i, 64), first + lo:first + hi] = (a * (b / (1.0 + jnp.exp(-b)))).astype(BF)
            return 0
        lax.fori_loop(0, T // 64, body, 0)

    sides = ((part, ra, st, rb, rs0, None), (part1, ra1, st1, rb1, rs1, second))

    def to_partner(q, d, j):
        prt, r_a, _, _, sems, _ = sides[q]
        bx = lax.rem(x + d, n_x)
        return rs_copy(prt.at[bx * 2 + 1 - c, :, pl.ds(j * w_j, w_j)], r_a.at[d, :, pl.ds(j * w_j, w_j)],
                       partner, sems[0].at[d, j], sems[1].at[d, j])

    def across(q, d, j):
        _, _, stage, r_b, sems, _ = sides[q]
        return rs_copy(stage.at[d - 1, :, pl.ds(j * w_j, w_j)], r_b.at[d - 1, :, pl.ds(j * w_j, w_j)],
                       lax.rem(x + d, n_x) * 2 + c, sems[2].at[d, j], sems[3].at[d, j])

    def down(q, j):
        prt, cond = sides[q][0], sides[q][5]

        @when(cond)
        def _():
            def body(r, _):
                val = jnp.dot(hid[q, rows_of(r), :], db[j], preferred_element_type=F32).astype(BF)
                for src in range(n_f):
                    lo = (src % per_block) * slotw + j * 128
                    prt[src // per_block, rows_of(r), lo:lo + 128] = val[:, src * 128:(src + 1) * 128]
                return 0
            lax.fori_loop(0, R, body, 0)
        for d in list(range(1, n_x)) + [0]:
            go(to_partner(q, d, j), cond)

    def combine(q, j):
        prt, r_a, stage, _, _, cond = sides[q]
        for d in range(1, n_x):
            bx = lax.rem(x + d, n_x)
            recv(to_partner(q, d, j), cond)

            @when(cond)
            def _():
                stage[d - 1, :, cols_of(j)] = (prt[bx * 2 + c, :, cols_of(j)].astype(F32)
                                               + r_a[d, :, cols_of(j)].astype(F32)).astype(BF)
            go(across(q, d, j), cond)

    def finish(q, j):
        prt, r_a, _, r_b, _, cond = sides[q]
        base = (mw, mw1)[q]
        recv(to_partner(q, 0, j), cond)
        for d in range(1, n_x):
            recv(across(q, d, j), cond)

        @when(cond)
        def _():
            total = prt[t, :, cols_of(j)].astype(F32) + r_a[0, :, cols_of(j)].astype(F32)
            for d in range(1, n_x):
                total = total + r_b[d - 1, :, cols_of(j)].astype(F32)
            val = (base[t, :, cols_of(j)].astype(F32) + total).astype(BF)
            if q == 0:
                o_ref[:, cols_of(j)] = val
            else:
                fin[j] = val
        if q == 1:
            go(fin_copy(j, guest), cond)

    def inner_part():
        open_copies.append([])
        for r in range(R):
            ag_forward(mw, r, agm)
        pump(1)
        for r in range(R):
            ag_finish(mw, r, agm)
            norm_rows(mw, cg, r, xn)
            pump(1)
        lift[0:16, :] = jnp.zeros((16, lift.shape[1]), BF)
        swit[0:16, :] = jnp.zeros((16, swit.shape[1]), BF)
        n_c = len(chunks)
        for k in range(n_c):
            if k == n_c - 1:
                for r in range(R):
                    recv(token_copy(r, guest), second)
                    ag_start(mw1, r, agn, second)
            arrive_all("ff%d" % k)
            widen(ub, xn, lift, k)
            pump(1)
            widen(sb, xn, swit, k)
            pump(1)
            conv(0, k)
            pump(1)
        for r in range(R):
            ag_forward(mw1, r, agn, second)
        for r in range(R):
            ag_finish(mw1, r, agn, second)
            when(second)(lambda: norm_rows(mw1, cg, r, xn1))
            pump(1)
        for k in range(n_c):
            when(second)(lambda: widen(ub, xn1, lift, k))
            pump(1)
            when(second)(lambda: widen(sb, xn1, swit, k))
            pump(1)
            when(second)(lambda: conv(1, k))
            pump(1)
        for j in range(n_j):
            arrive_all("down%d" % j)
            down(1, j)
            down(0, j)
            combine(1, j)
            combine(0, j)
            pump(1)
            if j > 0:
                finish(1, j - 1)
                finish(0, j - 1)
            pump(1)
        finish(1, n_j - 1)
        finish(0, n_j - 1)
        drain()
        open_copies.pop()

    kept = dict(state)
    pl.when(is_end)(end_part)
    state.update(kept)
    pl.when(inner)(inner_part)
    drain()


def on_device(cfg, inputs, mixer_gain, query_weight, key_weight, value_weight, gate_weight, head_gain,
              out_weight, channel_gain, up_weight, switch_weight, filter_up, filter_switch, down_weight):
    n_g, n_f, n_t = cfg
    n_x = n_t // 2
    T, bw = inputs.shape
    D = bw * n_t
    fr, width = query_weight.shape
    heads = width // HEAD
    F = up_weight.shape[1]
    slotw = out_weight.shape[1]
    half = HEAD // 2
    per_block = bw // slotw
    n_j = slotw // 128
    assert n_f >= 4 and slotw % 128 == 0 and bw % slotw == 0 and (n_j == 1 or per_block == 1)
    frequency = 10000.0 ** (-jnp.arange(half, dtype=F32) * 2.0 / HEAD)
    angles = jnp.arange(T, dtype=jnp.int32).astype(F32)[:, None] * frequency[None, :]
    cosine, sine = jnp.cos(angles), jnp.sin(angles)
    cos2 = jnp.concatenate([cosine, cosine], axis=1)
    sin2 = jnp.concatenate([-sine, sine], axis=1)
    ids = (lax.axis_index("tp") * heads + jnp.arange(heads, dtype=jnp.int32)).astype(F32)
    rate = jnp.broadcast_to(jnp.log1p(-jnp.exp2(-5.0 - ids))[:, None], (heads, 128))

    chunks = hidden_chunks(F)
    span = max(hi - lo for lo, hi in chunks)
    n_p = 3 + 2 * len(chunks) + n_j
    R = T // 256
    dma = pltpu.SemaphoreType.DMA
    anyspec = pl.BlockSpec(memory_space=pl.ANY)
    vspec = pl.BlockSpec(memory_space=pltpu.VMEM)
    act = pltpu.VMEM((n_t, T, bw), BF)
    flat = pltpu.VMEM((T, D), BF)
    xblk = pltpu.VMEM((n_x, T, bw), BF)
    yblk = pltpu.VMEM((n_x - 1, T, bw), BF)
    scratch = [
        pltpu.VMEM((D, 4 * width), BF),
        pltpu.VMEM((n_f,) + out_weight.shape, BF),
        pltpu.VMEM((D, F), BF),
        pltpu.VMEM((D, F), BF),
        pltpu.VMEM((n_j, F, n_f * 128), BF),
        act, flat, flat,
        pltpu.VMEM((T, width), BF), pltpu.VMEM((T, width), BF),
        pltpu.VMEM((T, width), BF), pltpu.VMEM((T, width), BF),
        pltpu.VMEM((T, width), BF),
        act, xblk, yblk, yblk,
        act, act,
        pltpu.VMEM((T + 16, span), BF), pltpu.VMEM((T + 16, span), BF), pltpu.VMEM((2, T, F), BF),
        act, xblk, yblk, yblk,
        pltpu.VMEM((n_j, T, per_block * 128), BF),
        dma((8 + n_j,)),
        dma((n_p, 2 * n_f)), dma((n_p, n_f)), dma((n_p, n_f * n_g)), dma((n_p, n_f * n_g)),
        dma((R,)), dma((R,)), dma((n_j,)), dma((n_j,)),
    ] + [dma((n_x, R))] * 16 + [dma((n_x, n_j))] * 8
    flops = 2 * T * (D * 4 * width + width * D + 3 * D * F)
    call = pl.pallas_call(
        functools.partial(kernel, cfg),
        out_shape=jax.ShapeDtypeStruct((T, bw), BF),
        in_specs=[anyspec, vspec, anyspec, anyspec, anyspec, anyspec, vspec, anyspec, vspec, anyspec, anyspec,
                  vspec, vspec, anyspec, vspec, vspec, vspec],
        out_specs=vspec,
        scratch_shapes=scratch,
        compiler_params=pltpu.CompilerParams(
            collective_id=0, has_side_effects=True, vmem_limit_bytes=67043328),
        cost_estimate=pl.CostEstimate(flops=flops, bytes_accessed=2 * (D * F * 3), transcendentals=0),
    )
    return call(inputs, mixer_gain[None, :], query_weight, key_weight, value_weight, gate_weight,
                head_gain[None, :], out_weight, channel_gain[None, :], up_weight, switch_weight,
                filter_up, filter_switch, down_weight, cos2, sin2, rate)


def solution(mesh):
    cfg = (mesh.shape["grp"], mesh.shape["fs"], mesh.shape["tp"])
    return jax.shard_map(
        functools.partial(on_device, cfg),
        mesh=mesh,
        in_specs=(
            P(("grp", "fs"), "tp"),
            P(),
            P("fs", "tp"),
            P("fs", "tp"),
            P("fs", "tp"),
            P("fs", "tp"),
            P("tp"),
            P("tp", "fs"),
            P(),
            P("fs", "tp"),
            P("fs", "tp"),
            P(None, "tp"),
            P(None, "tp"),
            P("tp", "fs"),
        ),
        out_specs=P(("grp", "fs"), "tp"),
        check_vma=False,
    )
```

time: 236 us -> 249 us (1.055); the launches traced: 236 us -> 245 us
  Pallas kernels: 230 us -> 240 us
    pallas_call x1, Pallas kernels: 230 us -> 240 us  [on_device(): call(inputs, mixer_gain[None, :], query_weight, key_weight, value_weight,...]
where the time goes in v1:
time: 249 us; the launch traced here: 245 us
  Pallas kernels  240 us (96%)
  local copies, waits for them, and re-layouts  2.68 us (1%)
  other arithmetic  2.62 us (1%)
    pallas_call x1, Pallas kernels, on_device(): call(inputs, mixer_gain[None, :], query_weight, key_weight, value_weight,...  240 us

profile of v1, /device:TPU:3, one launch (start us, length us, event | category | flops | bytes accessed | tf_op | source)
XLA Modules:
  0.0 244.8 jit_solution(10726273870024962529)
XLA Ops:
  0.0 1.5 fusion
  1.5 1.1 pad_maximum_fusion
  2.6 0.6 broadcast_in_dim.20.ld_ref
  3.2 239.5 %shard_map.136 = bf16[768,512]{1,0:T(8,128)(2,1)} custom-call(bf16[768,512]{1,0:T(8,128)(2,1)} %x_hbm.1, f32[1,2048]{1,0:T(1,128)} %bitcast.3, bf16[512,256]{1,0:T(8,128)(2,1)} %q_hbm.1, bf16[512,256]{1,0:T(8,128)(2,1)} %k_hbm.1, bf16[512,256]{1,0:T(8,128)(2,1)} %v_hbm.1, bf16[512,256]{1,0:T(8,128)(2,1)} %g_hbm.1, f32[1,256]{1,0:T(1,128)} %bitcast.5, ...), custom_call_target="tpu_custom_call" | custom-call | flops 17314086912 | bytes 17301504 | tf_op jit(solution)/shard_map/pallas_call | solution.py:601
  242.8 2.1 copy.16
  (3 shorter events, 0.0 us)

commit v2 on v1

--- a/solution.py
+++ b/solution.py
@@ -12,7 +12,12 @@
 MESH = pl.DeviceIdType.MESH
 BF = jnp.bfloat16
 F32 = jnp.float32
-LEAD = 3
+EARLY = 4
+HALVED = 2
+
+
+def qkvg_pieces(rows):
+    return 4 if rows % 64 == 0 and rows > 64 else 1
 
 
 def hidden_chunks(hidden):
@@ -100,7 +105,7 @@
 
     def add_rows(name, buf, slotted, shard, cols=None):
         half = shard // n_g
-        count = 2 if name == "qkvg" and half % 32 == 0 else 1
+        count = qkvg_pieces(half) if name == "qkvg" else 1
         size = half // count
         for j in range(count):
             def ref(src, owner, j=j):
@@ -149,26 +154,38 @@
 
     def own(p):
         for way in (0, 1):
-            go(z_copy(p, z, 0, way), onward(p, way))
-        if p >= first_ff:
+            ahead = onward(p, way)
+            go(z_copy(p, z, 0, way), jnp.logical_and(ahead, inner) if p >= first_ff else ahead)
+
+    def whole(p):
+        return not n_p - n_j <= p < n_p - n_j + min(HALVED, n_j - 1)
+
+    def own_from_end(p):
+        go(pltpu.make_async_remote_copy(
+            src_ref=pieces[p][1](z, grp), dst_ref=pieces[p][1](z, grp), send_sem=ys.at[p, z * n_g],
+            recv_sem=zr.at[p, z], device_id=(grp, host, t), device_id_type=MESH), is_end)
+        if whole(p):
             for d in range(1, n_g):
                 go(other_half(p, d), is_end)
 
-    def event(p, s):
+    def event(p, s, kind):
         feed = p >= first_ff
         for way in (0, 1):
             src = z - s if way == 0 else z + s
             here = (src >= 0) if way == 0 else (src < n_f)
             if feed:
                 here = jnp.logical_and(here, inner)
+            far = True if s > 1 else z != (1 if way == 0 else n_f - 2)
+            if kind == "near":
+                here = jnp.logical_and(here, jnp.logical_not(far))
+            if kind == "mid":
+                here = jnp.logical_and(here, far)
             safe = jnp.clip(src, 0, n_f - 1)
             recv(z_copy(p, safe, s, way), here)
             go(z_copy(p, safe, s, way), jnp.logical_and(here, onward(p, way)))
-            share = here
-            if feed and s == 1:
-                share = jnp.logical_and(here, z != (1 if way == 0 else n_f - 2))
-            for d in range(1, n_g):
-                go(y_copy(p, safe, d), share)
+            if kind != "near" or not whole(p):
+                for d in range(1, n_g):
+                    go(y_copy(p, safe, d), jnp.logical_and(here, far) if whole(p) else here)
 
     def arrive(p):
         for s in range(1, n_f):
@@ -182,7 +199,22 @@
                     device_id=(owner, z, t), device_id_type=MESH).wait_recv()
 
     state = {"own": 0, "ev": 0}
-    order = [(p, s) for p in range(n_p) for s in range(1, n_f - 1 if p >= first_ff else n_f)]
+    order = [(0, p, s, None) for s in range(1, n_f) for p in range(first_ff)]
+
+    def when_due(p, s, kind):
+        i, k = p - first_ff, p - (n_p - n_j)
+        if kind == "mid":
+            return 123 + 4 * k if k >= 0 else (71.2 + 5.6 * i if i < 3 else (93.6, 103.5, 113.3)[min(i, 5) - 3])
+        near = (146.5, 150.5, 158.3, 166)[min(k, 3)] if k >= 0 else (75.2 + 11.2 * i if i < EARLY else 97 + 9.2 * i)
+        if kind == "near":
+            return near
+        return near + (12.5 - 0.7 * i if i < EARLY else 4.5) + 6 * (s - 2)
+
+    later = []
+    for p in range(first_ff, n_p):
+        later += [(when_due(p, 1, kind), p, 1, kind) for kind in ("mid", "near")]
+        later += [(when_due(p, s, "far"), p, s, "far") for s in range(2, n_f - 1)]
+    order += sorted(later)
 
     def send_own(upto):
         while state["own"] < min(upto, n_p):
@@ -192,15 +224,21 @@
     def pump(count=1):
         for _ in range(count):
             if state["ev"] < len(order):
-                p, s = order[state["ev"]]
-                send_own(p + LEAD)
-                event(p, s)
+                _, p, s, kind = order[state["ev"]]
+                event(p, s, kind)
+                if (p, s) == (first_ff - 1, 1):
+                    send_own(first_ff + 3)
+                if kind == "near":
+                    send_own(p + 4 if p - first_ff < 3 else n_p)
                 state["ev"] += 1
 
+    def pump_to(due):
+        while state["ev"] < len(order) and order[state["ev"]][0] <= due:
+            pump()
+
     def arrive_all(name):
-        last = max(i for i, pc in enumerate(pieces) if pc[0] == name)
-        while state["ev"] < len(order) and order[state["ev"]][0] <= last:
-            pump()
+        last = max(i for i, e in enumerate(order) if pieces[e[1]][0] == name)
+        pump(max(0, last + 1 - state["ev"]))
         for i, pc in enumerate(pieces):
             if pc[0] == name:
                 arrive(i)
@@ -281,20 +319,30 @@
                                         + ra[d, rows_of(r), :].astype(F32)).astype(BF)
             begin(across(d, r))
 
-        work = [(d, r) for d in range(1, n_x) for r in range(R)]
-        prev = None
-        for d, r in work + [(0, r) for r in range(R)]:
-            bx = lax.rem(x + d, n_x)
-            product(ho, ob, part, bx * 2 + 1 - c, r)
-            begin(to_partner(d, r))
-            product(ho, ob, part, bx * 2 + c, r)
-            if prev is not None and prev[0] > 0:
-                combine(*prev)
-            prev = (d, r)
-            if r % 2 == 1:
-                pump(1)
         for r in range(R):
-            pump(1)
+            project(r)
+            for h in range(heads):
+                retain(h, r)
+            if r == 0:
+                arrive_all("out")
+            for d in range(1, n_x):
+                bx = lax.rem(x + d, n_x)
+                product(ho, ob, part, bx * 2 + 1 - c, r)
+                begin(to_partner(d, r))
+                product(ho, ob, part, bx * 2 + c, r)
+            if r > 0:
+                for d in range(1, n_x):
+                    combine(d, r - 1)
+            pump_to((0, 0, 75.3)[min(r, 2)])
+        for r in range(R):
+            product(ho, ob, part, x * 2 + 1 - c, r)
+            begin(to_partner(0, r))
+            if r == 0:
+                for d in range(1, n_x):
+                    combine(d, R - 1)
+            product(ho, ob, part, x * 2 + c, r)
+        for r in range(R):
+            pump_to((77, 86.5, 89)[min(r, 2)])
             to_partner(0, r).wait_recv()
             total = part[t, rows_of(r), :].astype(F32) + ra[0, rows_of(r), :].astype(F32)
             for d in range(1, n_x):
@@ -310,17 +358,21 @@
         ag_start(xw, r, agx)
     for cp in local[1:]:
         cp.wait()
-    send_own(2)
-    pump(1)
+    send_own(first_ff)
+    for p in range(first_ff):
+        for d in range(1, n_g):
+            go(other_half(p, d), is_end)
+    early = min(first_ff + EARLY, n_p - n_j)
+    for p in range(first_ff, early):
+        own_from_end(p)
     for r in range(R):
+        pump(2 if r < 2 else 1)
         ag_forward(xw, r, agx)
-    pump(1)
     for r in range(R):
         ag_finish(xw, r, agx)
         norm_rows(xw, mg, r, xn)
         pump(1)
     arrive_all("qkvg")
-    send_own(5)
 
     def project(r):
         rows = rows_of(r)
@@ -335,29 +387,22 @@
                 dst[rows, h * HEAD:(h + 1) * HEAD] = (
                     part_h * cos_ref[rows, :] + pltpu.roll(part_h, HEAD // 2, 1) * sin_ref[rows, :]).astype(BF)
 
-    for r in range(R):
-        project(r)
-        pump(1)
-    for h in range(heads):
+    def retain(h, r):
         cols = slice(h * HEAD, (h + 1) * HEAD)
-        for r in range(R):
-            span = (r + 1) * RC
-            qh = qr[r * RC:(r + 1) * RC, cols]
-            scores = lax.dot_general(qh, kr[0:span, cols], (((1,), (1,)), ((), ())),
-                                     preferred_element_type=F32)
-            gap = (r * RC + lax.broadcasted_iota(jnp.int32, (RC, span), 0)
-                   - lax.broadcasted_iota(jnp.int32, (RC, span), 1))
-            causal = gap >= 0
-            rate = ld_ref[h:h + 1, 0:1]
-            fade = jnp.where(causal, jnp.exp(rate * jnp.where(causal, gap, 0).astype(F32)), 0.0)
-            weights = (scores * HEAD ** (-0.5) * fade).astype(BF)
-            kept = jnp.dot(weights, vr[0:span, cols], preferred_element_type=F32)
-            kept = kept * lax.rsqrt(jnp.mean(kept * kept, axis=-1, keepdims=True) + EPS)
-            gate = gr[r * RC:(r + 1) * RC, cols].astype(F32)
-            ho[r * RC:(r + 1) * RC, cols] = (kept * hg[:, cols] * (gate / (1.0 + jnp.exp(-gate)))).astype(BF)
-            if r != 1:
-                pump(1)
-    arrive_all("out")
+        span = (r + 1) * RC
+        qh = qr[r * RC:(r + 1) * RC, cols]
+        scores = lax.dot_general(qh, kr[0:span, cols], (((1,), (1,)), ((), ())),
+                                 preferred_element_type=F32)
+        gap = (r * RC + lax.broadcasted_iota(jnp.int32, (RC, span), 0)
+               - lax.broadcasted_iota(jnp.int32, (RC, span), 1))
+        causal = gap >= 0
+        rate = ld_ref[h:h + 1, 0:1]
+        fade = jnp.where(causal, jnp.exp(rate * jnp.where(causal, gap, 0).astype(F32)), 0.0)
+        weights = (scores * HEAD ** (-0.5) * fade).astype(BF)
+        kept = jnp.dot(weights, vr[0:span, cols], preferred_element_type=F32)
+        kept = kept * lax.rsqrt(jnp.mean(kept * kept, axis=-1, keepdims=True) + EPS)
+        gate = gr[r * RC:(r + 1) * RC, cols].astype(F32)
+        ho[r * RC:(r + 1) * RC, cols] = (kept * hg[:, cols] * (gate / (1.0 + jnp.exp(-gate)))).astype(BF)
 
     def token_copy(r, dest):
         return pltpu.make_async_remote_copy(
@@ -381,7 +426,8 @@
 
     def end_part():
         open_copies.append([])
-        send_own(n_p)
+        for p in range(early, n_p):
+            own_from_end(p)
         for j in range(n_j):
             fin_copy(j, host).wait_recv()
             o_ref[:, cols_of(j)] = fin[j]
@@ -476,52 +522,79 @@
 
     def inner_part():
         open_copies.append([])
+        n_c = len(chunks)
+        lift[0:16, :] = jnp.zeros((16, lift.shape[1]), BF)
+        swit[0:16, :] = jnp.zeros((16, swit.shape[1]), BF)
+        pump_to(98)
         for r in range(R):
             ag_forward(mw, r, agm)
-        pump(1)
+            pump_to((103.6, 108.9, 111)[min(r, 2)])
         for r in range(R):
             ag_finish(mw, r, agm)
             norm_rows(mw, cg, r, xn)
-            pump(1)
-        lift[0:16, :] = jnp.zeros((16, lift.shape[1]), BF)
-        swit[0:16, :] = jnp.zeros((16, swit.shape[1]), BF)
-        n_c = len(chunks)
-        for k in range(n_c):
-            if k == n_c - 1:
-                for r in range(R):
-                    recv(token_copy(r, guest), second)
-                    ag_start(mw1, r, agn, second)
+
+        def feed(q, k, between=lambda: None):
+            cond = sides[q][5]
+            lhs = (xn, xn1)[q]
+            when(cond)(lambda: widen(ub, lhs, lift, k))
+            between()
+            when(cond)(lambda: widen(sb, lhs, swit, k))
+            when(cond)(lambda: conv(q, k))
+
+        def token(r):
+            recv(token_copy(r, guest), second)
+            ag_start(mw1, r, agn, second)
+
+        arrive_all("ff0")
+        feed(0, 0, lambda: pump_to(113.5))
+        token(0)
+        pump_to(120)
+        if R > 2:
+            token(1)
+        pump_to(124)
+        for k in range(1, n_c - 1):
             arrive_all("ff%d" % k)
-            widen(ub, xn, lift, k)
-            pump(1)
-            widen(sb, xn, swit, k)
-            pump(1)
-            conv(0, k)
-            pump(1)
+            if k == 1:
+                token(R - 1)
+            feed(0, k, lambda: pump_to(132))
+        if n_c < 3:
+            token(R - 1)
         for r in range(R):
             ag_forward(mw1, r, agn, second)
+        pump_to(134)
         for r in range(R):
             ag_finish(mw1, r, agn, second)
             when(second)(lambda: norm_rows(mw1, cg, r, xn1))
-            pump(1)
-        for k in range(n_c):
-            when(second)(lambda: widen(ub, xn1, lift, k))
-            pump(1)
-            when(second)(lambda: widen(sb, xn1, swit, k))
-            pump(1)
-            when(second)(lambda: conv(1, k))
-            pump(1)
-        for j in range(n_j):
+        pump_to(135)
+        for k in range(n_c - 1):
+            feed(1, k, lambda: pump_to(139 if k == 0 else 143))
+            pump_to(143 if k == 0 else 150.6)
+        pump_to(151.5)
+        if n_c > 1:
+            arrive_all("ff%d" % (n_c - 1))
+            feed(0, n_c - 1, lambda: pump_to(156))
+            pump_to(159)
+        arrive_all("down0")
+        down(0, 0)
+        pump_to(160)
+
+        def between():
+            combine(0, 0)
+            pump_to(164)
+
+        feed(1, n_c - 1, between)
+        pump_to(167)
+        down(1, 0)
+        for j in range(1, n_j):
+            combine(1, j - 1)
             arrive_all("down%d" % j)
             down(1, j)
             down(0, j)
-            combine(1, j)
+            pump_to(1000)
             combine(0, j)
-            pump(1)
-            if j > 0:
-                finish(1, j - 1)
-                finish(0, j - 1)
-            pump(1)
+            finish(1, j - 1)
+            finish(0, j - 1)
+        combine(1, n_j - 1)
         finish(1, n_j - 1)
         finish(0, n_j - 1)
         drain()
@@ -558,7 +631,7 @@
 
     chunks = hidden_chunks(F)
     span = max(hi - lo for lo, hi in chunks)
-    n_p = 3 + 2 * len(chunks) + n_j
+    n_p = qkvg_pieces(fr // n_g) + 1 + 2 * len(chunks) + n_j
     R = T // 256
     dma = pltpu.SemaphoreType.DMA
     anyspec = pl.BlockSpec(memory_space=pl.ANY)

time: 249 us -> 202 us (0.81)
  Pallas kernels: 240 us -> 194 us
    pallas_call x1, Pallas kernels: 240 us -> 194 us  [on_device(): call(inputs, mixer_gain[None, :], query_weight, key_weight, value_weight,...]
where the time goes in v2:
time: 202 us; the launch traced here: 200 us
  Pallas kernels  194 us (96%)
  local copies, waits for them, and re-layouts  2.68 us (1%)
  other arithmetic  2.62 us (1%)
    pallas_call x1, Pallas kernels, on_device(): call(inputs, mixer_gain[None, :], query_weight, key_weight, value_weight,...  194 us

profile of v2, /device:TPU:3, one launch (start us, length us, event | category | flops | bytes accessed | tf_op | source)
XLA Modules:
  0.0 199.5 jit_solution(3912818162334694442)
XLA Ops:
  0.0 1.5 fusion
  1.5 1.1 pad_maximum_fusion
  2.6 0.6 broadcast_in_dim.20.ld_ref
  3.2 194.2 %shard_map.136 = bf16[768,512]{1,0:T(8,128)(2,1)} custom-call(bf16[768,512]{1,0:T(8,128)(2,1)} %x_hbm.1, f32[1,2048]{1,0:T(1,128)} %bitcast.3, bf16[512,256]{1,0:T(8,128)(2,1)} %q_hbm.1, bf16[512,256]{1,0:T(8,128)(2,1)} %k_hbm.1, bf16[512,256]{1,0:T(8,128)(2,1)} %v_hbm.1, bf16[512,256]{1,0:T(8,128)(2,1)} %g_hbm.1, f32[1,256]{1,0:T(1,128)} %bitcast.5, ...), custom_call_target="tpu_custom_call" | custom-call | flops 17314086912 | bytes 17301504 | tf_op jit(solution)/shard_map/pallas_call | solution.py:674
  197.5 2.1 %copy.16 = bf16[768,512]{1,0:T(8,128)(2,1)} copy(bf16[768,512]{1,0:T(8,128)(2,1)} %shard_map.136) | data formatting | bytes 1572864
  (3 shorter events, 0.0 us)

commit v3 on v2

--- a/solution.py
+++ b/solution.py
@@ -2,6 +2,7 @@
 
 import jax
 import jax.numpy as jnp
+import numpy as np
 from jax import lax
 from jax.experimental import pallas as pl
 from jax.experimental.pallas import tpu as pltpu
@@ -13,7 +14,6 @@
 BF = jnp.bfloat16
 F32 = jnp.float32
 EARLY = 4
-HALVED = 2
 
 
 def qkvg_pieces(rows):
@@ -28,10 +28,10 @@
 
 
 def kernel(cfg, x_hbm, mg, q_hbm, k_hbm, v_hbm, g_hbm, hg, ow_hbm, cg, up_hbm, sw_hbm, fu, fsw, dn_hbm,
-           cos_ref, sin_ref, ld_ref, o_ref, *scratch):
+           turn_hbm, ld_ref, o_ref, *scratch):
     (wq, ob, ub, sb, db, xw, xn, xn1, qr, kr, vr, gr, ho, part, ra, st, rb, mw, mw1, lift, swit, hid,
-     part1, ra1, st1, rb1, fin, loc, zs, zr, ys, yr, tks, tkr, fns, fnr) = scratch[:36]
-    agx, agm, agn, rsm, rs0, rs1 = [scratch[36 + 4 * i:40 + 4 * i] for i in range(6)]
+     part1, ra1, st1, rb1, fin, turn, loc, zs, zr, ys, yr, tks, tkr, fns, fnr) = scratch[:37]
+    agx, agm, agn, rsm, rs0, rs1 = [scratch[37 + 4 * i:41 + 4 * i] for i in range(6)]
     n_g, n_f, n_t = cfg
     n_x = n_t // 2
     grp, z, t = lax.axis_index("grp"), lax.axis_index("fs"), lax.axis_index("tp")
@@ -84,6 +84,7 @@
     for j in range(n_j):
         local.append(pltpu.make_async_copy(
             dn_hbm.at[:, pl.ds(j * 128, 128)], db.at[j, :, pl.ds(zcol, 128)], loc.at[8 + j]))
+    local.append(pltpu.make_async_copy(turn_hbm, turn, loc.at[8 + n_j]))
     for cp in local:
         cp.start()
 
@@ -135,17 +136,20 @@
             src_ref=ref, dst_ref=ref, send_sem=zs.at[p, 2 * step + way], recv_sem=zr.at[p, src],
             device_id=(grp, z + (1 if way == 0 else -1), t), device_id_type=MESH)
 
+    def y_slot(src, d):
+        return src * (n_g - 1) + d - 1
+
     def y_copy(p, src, d):
         ref = pieces[p][1](src, grp)
         return pltpu.make_async_remote_copy(
-            src_ref=ref, dst_ref=ref, send_sem=ys.at[p, src * n_g + d], recv_sem=yr.at[p, src * n_g + grp],
+            src_ref=ref, dst_ref=ref, send_sem=ys.at[p, y_slot(src, d)], recv_sem=yr.at[p, y_slot(src, n_g - d)],
             device_id=(lax.rem(grp + d, n_g), z, t), device_id_type=MESH)
 
     def other_half(p, d):
         owner = lax.rem(grp + d, n_g)
         ref = pieces[p][1](z, owner)
         return pltpu.make_async_remote_copy(
-            src_ref=ref, dst_ref=ref, send_sem=ys.at[p, z * n_g + d], recv_sem=yr.at[p, z * n_g + owner],
+            src_ref=ref, dst_ref=ref, send_sem=ys.at[p, y_slot(z, d)], recv_sem=yr.at[p, y_slot(z, d)],
             device_id=(grp, host, t), device_id_type=MESH)
 
     def onward(p, way):
@@ -158,11 +162,11 @@
             go(z_copy(p, z, 0, way), jnp.logical_and(ahead, inner) if p >= first_ff else ahead)
 
     def whole(p):
-        return not n_p - n_j <= p < n_p - n_j + min(HALVED, n_j - 1)
+        return not first_ff + EARLY <= p < n_p - n_j
 
     def own_from_end(p):
         go(pltpu.make_async_remote_copy(
-            src_ref=pieces[p][1](z, grp), dst_ref=pieces[p][1](z, grp), send_sem=ys.at[p, z * n_g],
+            src_ref=pieces[p][1](z, grp), dst_ref=pieces[p][1](z, grp), send_sem=zs.at[p, 0],
             recv_sem=zr.at[p, z], device_id=(grp, host, t), device_id_type=MESH), is_end)
         if whole(p):
             for d in range(1, n_g):
@@ -181,8 +185,9 @@
             if kind == "mid":
                 here = jnp.logical_and(here, far)
             safe = jnp.clip(src, 0, n_f - 1)
-            recv(z_copy(p, safe, s, way), here)
-            go(z_copy(p, safe, s, way), jnp.logical_and(here, onward(p, way)))
+            recv(z_copy(p, safe, min(s, n_f - 2), way), here)
+            if s < n_f - 1:
+                go(z_copy(p, safe, s, way), jnp.logical_and(here, onward(p, way)))
             if kind != "near" or not whole(p):
                 for d in range(1, n_g):
                     go(y_copy(p, safe, d), jnp.logical_and(here, far) if whole(p) else here)
@@ -194,8 +199,8 @@
                 owner = lax.rem(grp + d, n_g)
                 ref = pieces[p][1](src, owner)
                 pltpu.make_async_remote_copy(
-                    src_ref=ref, dst_ref=ref, send_sem=ys.at[p, src * n_g],
-                    recv_sem=yr.at[p, src * n_g + owner],
+                    src_ref=ref, dst_ref=ref, send_sem=ys.at[p, y_slot(src, d)],
+                    recv_sem=yr.at[p, y_slot(src, d)],
                     device_id=(owner, z, t), device_id_type=MESH).wait_recv()
 
     state = {"own": 0, "ev": 0}
@@ -204,11 +209,13 @@
     def when_due(p, s, kind):
         i, k = p - first_ff, p - (n_p - n_j)
         if kind == "mid":
-            return 123 + 4 * k if k >= 0 else (71.2 + 5.6 * i if i < 3 else (93.6, 103.5, 113.3)[min(i, 5) - 3])
-        near = (146.5, 150.5, 158.3, 166)[min(k, 3)] if k >= 0 else (75.2 + 11.2 * i if i < EARLY else 97 + 9.2 * i)
+            if k >= 0:
+                return (124, 148.3, 156.1, 163.9)[min(k, 3)]
+            return 71.2 + 5.6 * i if i < 3 else (93.6, 109.2, 119.5)[min(i, 5) - 3]
+        near = 142.2 + 7.8 * k if k >= 0 else 75.2 + 11.2 * i if i < EARLY else 130.2 + 4.2 * (i - EARLY)
         if kind == "near":
             return near
-        return near + (12.5 - 0.7 * i if i < EARLY else 4.5) + 6 * (s - 2)
+        return near + (12.5 - 0.7 * i if i < EARLY else 6.4 if k < 0 else 6) + 6 * (s - 2)
 
     later = []
     for p in range(first_ff, n_p):
@@ -252,14 +259,14 @@
     def ag_start(buf, r, sems, cond=None):
         s1, r1, s2, r2 = sems
         for d in range(1, n_x):
-            go(ag_copy(buf, x, r, lax.rem(x + d, n_x) * 2 + c, s1.at[d, r], r1.at[x, r]), cond)
+            go(ag_copy(buf, x, r, lax.rem(x + d, n_x) * 2 + c, s1.at[d - 1, r], r1.at[x, r]), cond)
         go(ag_copy(buf, x, r, partner, s2.at[x, r], r2.at[x, r]), cond)
 
     def ag_forward(buf, r, sems, cond=None):
         s1, r1, s2, r2 = sems
         for d in range(1, n_x):
             sx = lax.rem(x + d, n_x)
-            recv(ag_copy(buf, sx, r, partner, s1.at[d, r], r1.at[sx, r]), cond)
+            recv(ag_copy(buf, sx, r, partner, s1.at[d - 1, r], r1.at[sx, r]), cond)
             go(ag_copy(buf, sx, r, partner, s2.at[sx, r], r2.at[sx, r]), cond)
 
     def ag_finish(buf, r, sems, cond=None):
@@ -304,7 +311,7 @@
 
         def across(d, r):
             return rs_copy(st.at[d - 1, rows_of(r), :], rb.at[d - 1, rows_of(r), :],
-                           lax.rem(x + d, n_x) * 2 + c, s2.at[d, r], r2.at[d, r])
+                           lax.rem(x + d, n_x) * 2 + c, s2.at[d - 1, r], r2.at[d - 1, r])
 
         sends = []
 
@@ -377,6 +384,11 @@
     def project(r):
         rows = rows_of(r)
         lhs = xn[rows, :]
+        both = turn[rows, :]
+        swapped = pltpu.roll(both, HEAD // 2, 1)
+        first_half = lax.broadcasted_iota(jnp.int32, (RC, HEAD), 1) < HEAD // 2
+        cosine = jnp.where(first_half, both, swapped)
+        sine = jnp.where(first_half, -swapped, both)
         for i, dst in enumerate((qr, kr, vr, gr)):
             val = jnp.dot(lhs, wq[:, i * width:(i + 1) * width], preferred_element_type=F32).astype(BF)
             if i >= 2:
@@ -385,7 +397,7 @@
             for h in range(heads):
                 part_h = val[:, h * HEAD:(h + 1) * HEAD].astype(F32)
                 dst[rows, h * HEAD:(h + 1) * HEAD] = (
-                    part_h * cos_ref[rows, :] + pltpu.roll(part_h, HEAD // 2, 1) * sin_ref[rows, :]).astype(BF)
+                    part_h * cosine + pltpu.roll(part_h, HEAD // 2, 1) * sine).astype(BF)
 
     def retain(h, r):
         cols = slice(h * HEAD, (h + 1) * HEAD)
@@ -396,7 +408,7 @@
         gap = (r * RC + lax.broadcasted_iota(jnp.int32, (RC, span), 0)
                - lax.broadcasted_iota(jnp.int32, (RC, span), 1))
         causal = gap >= 0
-        rate = ld_ref[h:h + 1, 0:1]
+        rate = ld_ref[pl.ds(t * heads + h, 1), 0:1]
         fade = jnp.where(causal, jnp.exp(rate * jnp.where(causal, gap, 0).astype(F32)), 0.0)
         weights = (scores * HEAD ** (-0.5) * fade).astype(BF)
         kept = jnp.dot(weights, vr[0:span, cols], preferred_element_type=F32)
@@ -471,7 +483,7 @@
     def across(q, d, j):
         _, _, stage, r_b, sems, _ = sides[q]
         return rs_copy(stage.at[d - 1, :, pl.ds(j * w_j, w_j)], r_b.at[d - 1, :, pl.ds(j * w_j, w_j)],
-                       lax.rem(x + d, n_x) * 2 + c, sems[2].at[d, j], sems[3].at[d, j])
+                       lax.rem(x + d, n_x) * 2 + c, sems[2].at[d - 1, j], sems[3].at[d - 1, j])
 
     def down(q, j):
         prt, cond = sides[q][0], sides[q][5]
@@ -556,41 +568,41 @@
             arrive_all("ff%d" % k)
             if k == 1:
                 token(R - 1)
-            feed(0, k, lambda: pump_to(132))
+            feed(0, k, lambda: pump_to(131))
         if n_c < 3:
             token(R - 1)
         for r in range(R):
             ag_forward(mw1, r, agn, second)
-        pump_to(134)
+        pump_to(134.5)
         for r in range(R):
             ag_finish(mw1, r, agn, second)
             when(second)(lambda: norm_rows(mw1, cg, r, xn1))
         pump_to(135)
         for k in range(n_c - 1):
             feed(1, k, lambda: pump_to(139 if k == 0 else 143))
-            pump_to(143 if k == 0 else 150.6)
-        pump_to(151.5)
+            pump_to(143 if k == 0 else 150.3)
         if n_c > 1:
             arrive_all("ff%d" % (n_c - 1))
-            feed(0, n_c - 1, lambda: pump_to(156))
-            pump_to(159)
+            feed(0, n_c - 1, lambda: pump_to(152))
+            pump_to(156.2)
         arrive_all("down0")
         down(0, 0)
-        pump_to(160)
+        pump_to(158)
 
         def between():
             combine(0, 0)
-            pump_to(164)
+            pump_to(158)
 
         feed(1, n_c - 1, between)
-        pump_to(167)
+        pump_to(164)
         down(1, 0)
         for j in range(1, n_j):
             combine(1, j - 1)
+            pump_to(156.4 + 7.6 * j)
             arrive_all("down%d" % j)
             down(1, j)
             down(0, j)
-            pump_to(1000)
+            pump_to(158.2 + 7.6 * j)
             combine(0, j)
             finish(1, j - 1)
             finish(0, j - 1)
@@ -621,13 +633,11 @@
     per_block = bw // slotw
     n_j = slotw // 128
     assert n_f >= 4 and slotw % 128 == 0 and bw % slotw == 0 and (n_j == 1 or per_block == 1)
-    frequency = 10000.0 ** (-jnp.arange(half, dtype=F32) * 2.0 / HEAD)
-    angles = jnp.arange(T, dtype=jnp.int32).astype(F32)[:, None] * frequency[None, :]
-    cosine, sine = jnp.cos(angles), jnp.sin(angles)
-    cos2 = jnp.concatenate([cosine, cosine], axis=1)
-    sin2 = jnp.concatenate([-sine, sine], axis=1)
-    ids = (lax.axis_index("tp") * heads + jnp.arange(heads, dtype=jnp.int32)).astype(F32)
-    rate = jnp.broadcast_to(jnp.log1p(-jnp.exp2(-5.0 - ids))[:, None], (heads, 128))
+    frequency = np.float32(10000.0) ** (-np.arange(half, dtype=np.float32) * np.float32(2.0) / np.float32(HEAD))
+    angles = np.arange(T, dtype=np.float32)[:, None] * frequency[None, :]
+    table = np.concatenate([np.cos(angles), np.sin(angles)], axis=1)
+    rates = np.log1p(-np.exp2(-5.0 - np.arange(n_t * heads, dtype=np.float32)))
+    rates = np.broadcast_to(rates[:, None], (n_t * heads, 128)).astype(np.float32)
 
     chunks = hidden_chunks(F)
     span = max(hi - lo for lo, hi in chunks)
@@ -655,16 +665,19 @@
         pltpu.VMEM((T + 16, span), BF), pltpu.VMEM((T + 16, span), BF), pltpu.VMEM((2, T, F), BF),
         act, xblk, yblk, yblk,
         pltpu.VMEM((n_j, T, per_block * 128), BF),
-        dma((8 + n_j,)),
-        dma((n_p, 2 * n_f)), dma((n_p, n_f)), dma((n_p, n_f * n_g)), dma((n_p, n_f * n_g)),
+        pltpu.VMEM((T, HEAD), F32),
+        dma((9 + n_j,)),
+        dma((n_p, 2 * (n_f - 1))), dma((n_p, n_f)),
+        dma((n_p, n_f * (n_g - 1))), dma((n_p, n_f * (n_g - 1))),
         dma((R,)), dma((R,)), dma((n_j,)), dma((n_j,)),
-    ] + [dma((n_x, R))] * 16 + [dma((n_x, n_j))] * 8
+    ] + ([dma((n_x - 1, R))] + [dma((n_x, R))] * 3) * 3 + ([dma((n_x, R))] * 2 + [dma((n_x - 1, R))] * 2) + (
+        [dma((n_x, n_j))] * 2 + [dma((n_x - 1, n_j))] * 2) * 2
     flops = 2 * T * (D * 4 * width + width * D + 3 * D * F)
     call = pl.pallas_call(
         functools.partial(kernel, cfg),
         out_shape=jax.ShapeDtypeStruct((T, bw), BF),
         in_specs=[anyspec, vspec, anyspec, anyspec, anyspec, anyspec, vspec, anyspec, vspec, anyspec, anyspec,
-                  vspec, vspec, anyspec, vspec, vspec, vspec],
+                  vspec, vspec, anyspec, anyspec, vspec],
         out_specs=vspec,
         scratch_shapes=scratch,
         compiler_params=pltpu.CompilerParams(
@@ -673,7 +686,7 @@
     )
     return call(inputs, mixer_gain[None, :], query_weight, key_weight, value_weight, gate_weight,
                 head_gain[None, :], out_weight, channel_gain[None, :], up_weight, switch_weight,
-                filter_up, filter_switch, down_weight, cos2, sin2, rate)
+                filter_up, filter_switch, down_weight, jnp.asarray(table), jnp.asarray(rates))
 
 
 def solution(mesh):

time: 202 us -> 186 us (0.921)
  Pallas kernels: 194 us -> 181 us
  other arithmetic: 2.62 us -> 0 us
    pallas_call x1, Pallas kernels: 194 us -> 181 us  [on_device(): call(inputs, mixer_gain[None, :], query_weight, key_weight, value_weight,...]
where the time goes in v3:
time: 186 us; the launch traced here: 183 us
  Pallas kernels  181 us (97%)
  local copies, waits for them, and re-layouts  2.06 us (1%)
    pallas_call x1, Pallas kernels, on_device(): call(inputs, mixer_gain[None, :], query_weight, key_weight, value_weight,...  181 us

profile of v3, /device:TPU:3, one launch (start us, length us, event | category | flops | bytes accessed | tf_op | source)
XLA Modules:
  0.0 182.9 jit_solution(7892484297261544611)
XLA Ops:
  0.0 180.8 %shard_map.154 = bf16[768,512]{1,0:T(8,128)(2,1)} custom-call(bf16[768,512]{1,0:T(8,128)(2,1)} %x_hbm.1, f32[1,2048]{1,0:T(1,128)} %bitcast.3, bf16[512,256]{1,0:T(8,128)(2,1)} %q_hbm.1, bf16[512,256]{1,0:T(8,128)(2,1)} %k_hbm.1, bf16[512,256]{1,0:T(8,128)(2,1)} %v_hbm.1, bf16[512,256]{1,0:T(8,128)(2,1)} %g_hbm.1, f32[1,256]{1,0:T(1,128)} %bitcast.5, ...), custom_call_target="tpu_custom_call" | custom-call | flops 17314086912 | bytes 17301504 | tf_op jit(solution)/shard_map/pallas_call | solution.py:687
  180.8 2.1 %copy.18 = bf16[768,512]{1,0:T(8,128)(2,1)} copy(bf16[768,512]{1,0:T(8,128)(2,1)} %shard_map.154) | data formatting | bytes 1572864

commit v4 on v3

--- a/solution.py
+++ b/solution.py
@@ -128,6 +128,7 @@
                          pl.ds(pl.multiple_of(src * 128, 128), 128)]
         pieces.append(("down%d" % j, down_ref))
     n_p = len(pieces)
+    out_p = [pc[0] for pc in pieces].index("out")
     first_ff = min(i for i, pc in enumerate(pieces) if pc[0] == "ff0")
 
     def z_copy(p, src, step, way):
@@ -159,10 +160,19 @@
     def own(p):
         for way in (0, 1):
             ahead = onward(p, way)
-            go(z_copy(p, z, 0, way), jnp.logical_and(ahead, inner) if p >= first_ff else ahead)
+            go(z_copy(p, z, 0, way), jnp.logical_and(ahead, inner) if p >= out_p else ahead)
 
     def whole(p):
         return not first_ff + EARLY <= p < n_p - n_j
+
+    def straight(p):
+        return n_f == 4 and n_p - n_j <= p < n_p - n_j + min(2, n_j - 1)
+
+    def relay(p, src, way, d):
+        ref = pieces[p][1](src, lax.rem(grp + d, n_g))
+        return pltpu.make_async_remote_copy(
+            src_ref=ref, dst_ref=ref, send_sem=ys.at[p, y_slot(src, d)], recv_sem=yr.at[p, y_slot(src, d)],
+            device_id=(grp, z + (1 if way == 0 else -1), t), device_id_type=MESH)
 
     def own_from_end(p):
         go(pltpu.make_async_remote_copy(
@@ -180,15 +190,20 @@
             if feed:
                 here = jnp.logical_and(here, inner)
             far = True if s > 1 else z != (1 if way == 0 else n_f - 2)
-            if kind == "near":
+            if kind in ("near", "rest"):
                 here = jnp.logical_and(here, jnp.logical_not(far))
             if kind == "mid":
                 here = jnp.logical_and(here, far)
             safe = jnp.clip(src, 0, n_f - 1)
+            if kind == "rest":
+                for d in range(1, n_g):
+                    recv(relay(p, safe, way, d), here)
+                    go(relay(p, safe, way, d), jnp.logical_and(here, onward(p, way)))
+                continue
             recv(z_copy(p, safe, min(s, n_f - 2), way), here)
             if s < n_f - 1:
                 go(z_copy(p, safe, s, way), jnp.logical_and(here, onward(p, way)))
-            if kind != "near" or not whole(p):
+            if not (kind == "near" and whole(p)) and not (kind == "far" and straight(p)):
                 for d in range(1, n_g):
                     go(y_copy(p, safe, d), jnp.logical_and(here, far) if whole(p) else here)
 
@@ -196,30 +211,41 @@
         for s in range(1, n_f):
             src = lax.rem(z + s, n_f)
             for d in range(1, n_g):
-                owner = lax.rem(grp + d, n_g)
-                ref = pieces[p][1](src, owner)
-                pltpu.make_async_remote_copy(
+                ref = pieces[p][1](src, lax.rem(grp + d, n_g))
+                recv(pltpu.make_async_remote_copy(
                     src_ref=ref, dst_ref=ref, send_sem=ys.at[p, y_slot(src, d)],
                     recv_sem=yr.at[p, y_slot(src, d)],
-                    device_id=(owner, z, t), device_id_type=MESH).wait_recv()
+                    device_id=(lax.rem(grp + d, n_g), z, t), device_id_type=MESH),
+                    src != guest if straight(p) else None)
 
     state = {"own": 0, "ev": 0}
-    order = [(0, p, s, None) for s in range(1, n_f) for p in range(first_ff)]
+    order = []
+    for s in range(1, n_f):
+        order += [(0, p, s, None) for p in range(out_p)]
+        if s < 3:
+            order.append((0, out_p, 1, ("near", "mid")[s - 1]))
+    order += [(0, out_p, s, "far") for s in range(2, n_f)]
 
     def when_due(p, s, kind):
         i, k = p - first_ff, p - (n_p - n_j)
         if kind == "mid":
             if k >= 0:
-                return (124, 148.3, 156.1, 163.9)[min(k, 3)]
-            return 71.2 + 5.6 * i if i < 3 else (93.6, 109.2, 119.5)[min(i, 5) - 3]
-        near = 142.2 + 7.8 * k if k >= 0 else 75.2 + 11.2 * i if i < EARLY else 130.2 + 4.2 * (i - EARLY)
+                return (122.2, 141.5, 151, 155)[min(k, 3)]
+            return 71.2 + 5.6 * i if i < 3 else (93.2, 108.4, 118.2)[min(i, 5) - 3]
+        near = 142.2 + 7.8 * k if k >= 0 else 69.6 + 11.2 * i if i < EARLY else 130.2 + 4.2 * (i - EARLY)
+        if kind == "rest":
+            return near
+        if k >= 0:
+            near -= 3.9
         if kind == "near":
             return near
-        return near + (12.5 - 0.7 * i if i < EARLY else 6.4 if k < 0 else 6) + 6 * (s - 2)
+        if i < EARLY:
+            return (87.7, 98.9, 104.5, 114)[min(i, 3)] + 6 * (s - 2)
+        return near + (6.4 if k < 0 else 8) + 6 * (s - 2)
 
     later = []
     for p in range(first_ff, n_p):
-        later += [(when_due(p, 1, kind), p, 1, kind) for kind in ("mid", "near")]
+        later += [(when_due(p, 1, kind), p, 1, kind) for kind in ("mid", "near", "rest")[:3 if straight(p) else 2]]
         later += [(when_due(p, s, "far"), p, s, "far") for s in range(2, n_f - 1)]
     order += sorted(later)
 
@@ -233,10 +259,11 @@
             if state["ev"] < len(order):
                 _, p, s, kind = order[state["ev"]]
                 event(p, s, kind)
-                if (p, s) == (first_ff - 1, 1):
-                    send_own(first_ff + 3)
+                if (p, s) == (out_p - 1, 1):
+                    send_own(first_ff)
                 if kind == "near":
-                    send_own(p + 4 if p - first_ff < 3 else n_p)
+                    i = p - first_ff
+                    send_own(first_ff + (3 if i < 0 else 4 if i < 2 else 5 if i < 3 else n_p))
                 state["ev"] += 1
 
     def pump_to(due):
@@ -340,7 +367,7 @@
             if r > 0:
                 for d in range(1, n_x):
                     combine(d, r - 1)
-            pump_to((0, 0, 75.3)[min(r, 2)])
+            pump_to((71.3, 71.3, 75.3)[min(r, 2)])
         for r in range(R):
             product(ho, ob, part, x * 2 + 1 - c, r)
             begin(to_partner(0, r))
@@ -363,12 +390,17 @@
     local[0].wait()
     for r in range(R):
         ag_start(xw, r, agx)
-    for cp in local[1:]:
+    for cp in local[1:5]:
         cp.wait()
-    send_own(first_ff)
+    send_own(out_p)
+    local[5].wait()
+    for way in (0, 1):
+        go(z_copy(out_p, z, 0, way), jnp.logical_and(onward(out_p, way), is_end))
     for p in range(first_ff):
         for d in range(1, n_g):
             go(other_half(p, d), is_end)
+    for cp in local[6:]:
+        cp.wait()
     early = min(first_ff + EARLY, n_p - n_j)
     for p in range(first_ff, early):
         own_from_end(p)
@@ -545,12 +577,13 @@
             ag_finish(mw, r, agm)
             norm_rows(mw, cg, r, xn)
 
-        def feed(q, k, between=lambda: None):
+        def feed(q, k, between=lambda: None, later=lambda: None):
             cond = sides[q][5]
             lhs = (xn, xn1)[q]
             when(cond)(lambda: widen(ub, lhs, lift, k))
             between()
             when(cond)(lambda: widen(sb, lhs, swit, k))
+            later()
             when(cond)(lambda: conv(q, k))
 
         def token(r):
@@ -568,18 +601,20 @@
             arrive_all("ff%d" % k)
             if k == 1:
                 token(R - 1)
-            feed(0, k, lambda: pump_to(131))
+            feed(0, k, lambda: pump_to(125))
+        pump_to(131)
         if n_c < 3:
             token(R - 1)
         for r in range(R):
+            if r == R - 1:
+                pump_to(134.5)
             ag_forward(mw1, r, agn, second)
-        pump_to(134.5)
         for r in range(R):
             ag_finish(mw1, r, agn, second)
             when(second)(lambda: norm_rows(mw1, cg, r, xn1))
         pump_to(135)
         for k in range(n_c - 1):
-            feed(1, k, lambda: pump_to(139 if k == 0 else 143))
+            feed(1, k, lambda: pump_to(139 if k == 0 else 146.2), lambda: pump_to(141.6 if k == 0 else 147))
             pump_to(143 if k == 0 else 150.3)
         if n_c > 1:
             arrive_all("ff%d" % (n_c - 1))
@@ -588,27 +623,41 @@
         arrive_all("down0")
         down(0, 0)
         pump_to(158)
+        if n_j > 1:
+            arrive_all("down1")
+            down(0, 1)
+        combine(0, 0)
 
         def between():
-            combine(0, 0)
-            pump_to(158)
-
-        feed(1, n_c - 1, between)
-        pump_to(164)
-        down(1, 0)
-        for j in range(1, n_j):
-            combine(1, j - 1)
-            pump_to(156.4 + 7.6 * j)
-            arrive_all("down%d" % j)
-            down(1, j)
-            down(0, j)
-            pump_to(158.2 + 7.6 * j)
-            combine(0, j)
-            finish(1, j - 1)
-            finish(0, j - 1)
-        combine(1, n_j - 1)
-        finish(1, n_j - 1)
-        finish(0, n_j - 1)
+            pump_to(161.8)
+            if n_j > 1:
+                combine(0, 1)
+
+        feed(1, n_c - 1, between, lambda: pump_to(165.7))
+        rest = [(1, j) for j in range(n_j)] + [(0, j) for j in range(2, n_j)]
+        last, ended = [], []
+
+        def end(*items):
+            for item in items:
+                if item not in ended and item[1] < n_j:
+                    finish(*item)
+                    ended.append(item)
+
+        for q, j in rest:
+            if q == 1 and j > 1:
+                pump_to(1000 if j == n_j - 1 else 166)
+                if j == n_j - 1:
+                    end((0, 0), (1, 0))
+                arrive_all("down%d" % j)
+            down(q, j)
+            for item in last:
+                combine(*item)
+            last = [(q, j)]
+            if j == 2 and q == 0:
+                end((1, 1))
+        for item in last:
+            combine(*item)
+        end((0, 0), (1, 0), (0, 1), *rest)
         drain()
         open_copies.pop()
 

time: 186 us -> 174 us (0.935)
  Pallas kernels: 181 us -> 169 us
    pallas_call x1, Pallas kernels: 181 us -> 169 us  [on_device(): call(inputs, mixer_gain[None, :], query_weight, key_weight, value_weight,...]
where the time goes in v4:
time: 174 us; the launch traced here: 171 us
  Pallas kernels  169 us (97%)
  local copies, waits for them, and re-layouts  2.06 us (1%)
    pallas_call x1, Pallas kernels, on_device(): call(inputs, mixer_gain[None, :], query_weight, key_weight, value_weight,...  169 us

profile of v4, /device:TPU:3, one launch (start us, length us, event | category | flops | bytes accessed | tf_op | source)
XLA Modules:
  0.0 171.0 jit_solution(13192948218752431882)
XLA Ops:
  0.0 169.0 %shard_map.154 = bf16[768,512]{1,0:T(8,128)(2,1)} custom-call(bf16[768,512]{1,0:T(8,128)(2,1)} %x_hbm.1, f32[1,2048]{1,0:T(1,128)} %bitcast.3, bf16[512,256]{1,0:T(8,128)(2,1)} %q_hbm.1, bf16[512,256]{1,0:T(8,128)(2,1)} %k_hbm.1, bf16[512,256]{1,0:T(8,128)(2,1)} %v_hbm.1, bf16[512,256]{1,0:T(8,128)(2,1)} %g_hbm.1, f32[1,256]{1,0:T(1,128)} %bitcast.5, ...), custom_call_target="tpu_custom_call" | custom-call | flops 17314086912 | bytes 17301504 | tf_op jit(solution)/shard_map/pallas_call | solution.py:736
  169.0 2.1 %copy.18 = bf16[768,512]{1,0:T(8,128)(2,1)} copy(bf16[768,512]{1,0:T(8,128)(2,1)} %shard_map.154) | data formatting | bytes 1572864

commit v5 on v4

--- a/solution.py
+++ b/solution.py
@@ -240,8 +240,8 @@
         if kind == "near":
             return near
         if i < EARLY:
-            return (87.7, 98.9, 104.5, 114)[min(i, 3)] + 6 * (s - 2)
-        return near + (6.4 if k < 0 else 8) + 6 * (s - 2)
+            return (87.7, 98.9, 104.5, 113.4)[min(i, 3)] + 6 * (s - 2)
+        return near + (8 if k >= 0 else 4.7 if i == EARLY else 6.4) + 6 * (s - 2)
 
     later = []
     for p in range(first_ff, n_p):
@@ -645,6 +645,10 @@
 
         for q, j in rest:
             if q == 1 and j > 1:
+                if j == n_j - 1:
+                    for item in last:
+                        combine(*item)
+                    last = []
                 pump_to(1000 if j == n_j - 1 else 166)
                 if j == n_j - 1:
                     end((0, 0), (1, 0))

time: 174 us -> 176 us (1.011)
  Pallas kernels: 169 us -> 172 us
    pallas_call x1, Pallas kernels: 169 us -> 172 us  [on_device(): call(inputs, mixer_gain[None, :], query_weight, key_weight, value_weight,...]
where the time goes in v5:
time: 176 us; the launch traced here: 174 us
  Pallas kernels  172 us (98%)
  local copies, waits for them, and re-layouts  2.06 us (1%)
    pallas_call x1, Pallas kernels, on_device(): call(inputs, mixer_gain[None, :], query_weight, key_weight, value_weight,...  172 us

profile of v5, /device:TPU:3, one launch (start us, length us, event | category | flops | bytes accessed | tf_op | source)
XLA Modules:
  0.0 174.3 jit_solution(3207453659437426270)
XLA Ops:
  0.0 172.2 %shard_map.154 = bf16[768,512]{1,0:T(8,128)(2,1)} custom-call(bf16[768,512]{1,0:T(8,128)(2,1)} %x_hbm.1, f32[1,2048]{1,0:T(1,128)} %bitcast.3, bf16[512,256]{1,0:T(8,128)(2,1)} %q_hbm.1, bf16[512,256]{1,0:T(8,128)(2,1)} %k_hbm.1, bf16[512,256]{1,0:T(8,128)(2,1)} %v_hbm.1, bf16[512,256]{1,0:T(8,128)(2,1)} %g_hbm.1, f32[1,256]{1,0:T(1,128)} %bitcast.5, ...), custom_call_target="tpu_custom_call" | custom-call | flops 17314086912 | bytes 17301504 | tf_op jit(solution)/shard_map/pallas_call | solution.py:740
  172.2 2.1 %copy.18 = bf16[768,512]{1,0:T(8,128)(2,1)} copy(bf16[768,512]{1,0:T(8,128)(2,1)} %shard_map.154) | data formatting | bytes 1572864
